TPU v7x, 256 devices: a 4x2x16 block of a 4x16x16 slice. The times are simulated.
256 devices in a mesh: grp: 2 (over y), sp: 32 (over z, core), tp: 4 (over x).
Axes of the slice: x: 4, y: 2, z: 16, core: 2. Of those that a mesh axis runs over, the one named last changes fastest.
The devices are a block of a 4x16x16 slice.
Arguments:
- query_wide: bfloat16 [32768, 1024], P(('grp', 'sp'), 'tp'), parts along dimension 0, may hold values from -6 to 6
- key_wide: bfloat16 [32768, 1024], P(('grp', 'sp'), 'tp'), parts along dimension 0, may hold values from -6 to 6
- value_wide: bfloat16 [32768, 1024], P(('grp', 'sp'), 'tp'), parts along dimension 0, may hold values from -6 to 6
- decay_wide: float32 [32768, 8], P(('grp', 'sp'), 'tp'), parts along dimension 0, may hold values from -2 to 0, as said below
- query_narrow: bfloat16 [32768, 1024], P(('grp', 'sp'), 'tp'), parts along dimension 0, may hold values from -6 to 6
- key_narrow: bfloat16 [32768, 1024], P(('grp', 'sp'), 'tp'), parts along dimension 0, may hold values from -6 to 6
- value_narrow: bfloat16 [32768, 1024], P(('grp', 'sp'), 'tp'), parts along dimension 0, may hold values from -6 to 6
- decay_narrow: float32 [32768, 16], P(('grp', 'sp'), 'tp'), parts along dimension 0, may hold values from -2 to 0, as said below
- residual: bfloat16 [32768, 2048], P(('grp', 'sp', 'tp')), parts along dimension 0, may hold values from -6 to 6
- out_wide: bfloat16 [1024, 2048], P('tp'), may hold values from -0.125 to 0.125
- out_narrow: bfloat16 [1024, 2048], P('tp'), may hold values from -0.125 to 0.125
- norm_gain: float32 [2048], replicated, may hold values from 0.1 to 1.9
- routes: int32 [32768, 2], P(('grp', 'sp', 'tp')), parts along dimension 0, may hold values from 0 to 31, all different within a row; in each aligned block of 128 rows (0 to 127, 128 to 255, ...) at most 12 rows name the same one
- route_weights: float32 [32768, 2], P(('grp', 'sp', 'tp')), parts along dimension 0, may hold values from 0.1 to 1
- expert_gate: bfloat16 [32, 2048, 2048], P('sp', None, 'tp'), may hold values from -0.375 to 0.375
- expert_up: bfloat16 [32, 2048, 2048], P('sp', None, 'tp'), may hold values from -0.375 to 0.375
- expert_down: bfloat16 [32, 2048, 2048], P('sp', 'tp'), may hold values from -0.03125 to 0.03125
Outputs:
- layer_out: bfloat16 [32768, 2048], P(('grp', 'sp', 'tp')), parts along dimension 0
There are 2 independent parts, one for each index of `grp`. A program takes and returns all parts, laid end to end along the dimension named above; an argument that names none is the same for every part. Nothing has to cross between parts.
Inputs may be any that keep to these rules, and one draw needn't show every extreme that they name: `decay_wide`: every entry is negative. `decay_narrow`: every entry is negative. `routes`: each row names 2 different experts; on the rows of one device no expert is named more than 12 times, a bound that some block reaches.
All inputs are finite; a program needn't handle non-finite values.
Results may differ from a plain program's by a relative error of at most 0.018.
Values may be sent and summed in bfloat16 or wider, within the bound.
A program may use at most 128 MiB of HBM per device.

v0:
```python
import jax
import jax.numpy as jnp
from jax import lax
from jax.sharding import Mesh
from jax.sharding import PartitionSpec as P

HEAD_WIDE = 128
HEAD_NARROW = 64
TOP_K = 2
SP = ("sp_0", "sp_1")
GRP_SP = ("grp", "sp_0", "sp_1")
GRP_SP_TP = ("grp", "sp_0", "sp_1", "tp")


norm_eps = 1e-05
clamp_limit = 7.0
swish_alpha = 1.702
rotary_base = 10000.0


def filled_with(value, identity):
    return jax.tree.map(
        lambda a, e: jnp.broadcast_to(jnp.asarray(e, a.dtype), a.shape), value, identity
    )


def prefix_by_axis(value, axes, combine, identity):
    before = start = filled_with(value, identity)
    total = value
    for axis in reversed(axes):
        length, mine = (lax.axis_size(axis), lax.axis_index(axis))
        pieces = jax.tree.map(
            lambda part, kind: lax.all_gather(part.astype(kind), axis),
            total,
            jax.tree.map(lambda a: jnp.bfloat16 if a.dtype == jnp.float32 else a.dtype, value),
        )
        inside, total = (start, start)
        for k in range(length):
            passed = k < mine
            total = combine(
                total, jax.tree.map(lambda part, own: part[k].astype(own.dtype), pieces, value)
            )
            inside = jax.tree.map(lambda new, old: jnp.where(passed, new, old), total, inside)
        before = combine(inside, before)
    return before


def cut_along(value, dim, length):
    lengths = value.shape
    pieces = value.reshape(*lengths[:dim], length, lengths[dim] // length, *lengths[dim + 1 :])
    return jnp.moveaxis(pieces, dim, 0)


def sent_and_summed(value, axis, dim):
    pieces = cut_along(value, dim, lax.axis_size(axis))
    arrived = lax.all_to_all(pieces, axis, split_axis=0, concat_axis=0, tiled=True)
    return arrived.astype(jnp.float32).sum(axis=0)


def laid_out(pieces, dim):
    pieces = jnp.moveaxis(pieces, 0, dim)
    lengths = pieces.shape
    return pieces.reshape(*lengths[:dim], lengths[dim] * lengths[dim + 1], *lengths[dim + 2 :])


def turned_blocks(pieces, axes, order):
    inside = pieces.shape[1:]
    filled = pieces.reshape(*(lax.axis_size(a) for a in axes), *inside)
    for k in order:
        filled = lax.all_to_all(filled, axes[k], k, k, tiled=True)
    return filled.reshape(-1, *inside)


def core_and_chips(value, groups, order, split_dim, concat_dim):
    length = lax.axis_size(groups[0]) * lax.axis_size(groups[1])
    pieces = cut_along(value, split_dim, length)
    return laid_out(turned_blocks(pieces, groups, order), concat_dim)


def rotate(values, positions):
    half_width = values.shape[-1] // 2
    inverse = rotary_base ** (-jnp.arange(half_width, dtype=jnp.float32) / half_width)
    angles = positions[:, None] * inverse[None, :]
    cosine = jnp.cos(angles)[:, None, :]
    sine_part = jnp.sin(angles)[:, None, :]
    lower_half = values[..., :half_width]
    upper_half = values[..., half_width:]
    return jnp.concatenate(
        [
            lower_half * cosine - upper_half * sine_part,
            lower_half * sine_part + upper_half * cosine,
        ],
        axis=-1,
    )


def group_norm(output_heads):
    center = jnp.mean(output_heads, axis=-1, keepdims=True)
    spread = jnp.mean(jnp.square(output_heads - center), axis=-1, keepdims=True)
    return (output_heads - center) * lax.rsqrt(spread + norm_eps)


def local_terms(query_in, key_in, value_in, log_decay, head_width, positions):
    length = query_in.shape[0]
    attention_group_count = query_in.shape[1] // head_width
    query_heads = query_in.astype(jnp.float32).reshape(length, attention_group_count, head_width)
    key_heads = key_in.astype(jnp.float32).reshape(length, attention_group_count, head_width)
    query_f = rotate(query_heads, positions).astype(jnp.bfloat16).astype(jnp.float32)
    key_f = (
        (rotate(key_heads, positions) * head_width ** (-0.5))
        .astype(jnp.bfloat16)
        .astype(jnp.float32)
    )
    value_f = value_in.reshape(length, attention_group_count, head_width).astype(jnp.float32)
    cumulative = jnp.cumsum(log_decay, axis=0)
    steps_in = jnp.arange(length, dtype=jnp.int32)
    causal = steps_in[:, None] >= steps_in[None, :]
    gaps = cumulative.T[:, :, None] - cumulative.T[:, None, :]
    decay_grid = jnp.exp(jnp.where(causal[None], gaps, -jnp.inf))
    scores = jnp.einsum("thd,shd->hts", query_f, key_f) * decay_grid
    inner_part = jnp.einsum("hts,she->the", scores, value_f)
    total_log = cumulative[-1]
    weighted = key_f * jnp.exp(total_log[None, :] - cumulative)[:, :, None]
    state_local = jnp.einsum("shd,she->hde", weighted, value_f)
    return (query_f, cumulative, inner_part, total_log, state_local)


def finish(parts, state_in):
    query_f, cumulative, inner_part = (parts[0], parts[1], parts[2])
    carried_part = jnp.exp(cumulative)[:, :, None] * jnp.einsum("thd,hde->the", query_f, state_in)
    normed_heads = group_norm(inner_part + carried_part)
    return normed_heads.reshape(normed_heads.shape[0], -1).astype(jnp.bfloat16)


def combine(earlier, later):
    return (
        earlier[0] + later[0],
        jnp.exp(later[0])[:, None, None] * earlier[1] + later[1],
        earlier[2] + later[2],
        jnp.exp(later[2])[:, None, None] * earlier[3] + later[3],
    )


def activate(gate_pre, up_pre):
    gate_clip = jnp.minimum(gate_pre, clamp_limit)
    up_clip = jnp.clip(up_pre, -clamp_limit, clamp_limit)
    return gate_clip * jax.nn.sigmoid(swish_alpha * gate_clip) * (up_clip + 1.0)


def body(
    query_wide,
    key_wide,
    value_wide,
    decay_wide,
    query_narrow,
    key_narrow,
    value_narrow,
    decay_narrow,
    residual,
    out_wide,
    out_narrow,
    norm_gain,
    routes,
    route_weights,
    expert_gate,
    expert_up,
    expert_down,
):
    length = query_wide.shape[0]
    tp_count = lax.axis_size("tp")
    experts = lax.axis_size(SP)
    model_width = residual.shape[1]
    positions = (lax.axis_index(SP) * length + jnp.arange(length, dtype=jnp.int32)).astype(
        jnp.float32
    )
    wide_parts = local_terms(query_wide, key_wide, value_wide, decay_wide, HEAD_WIDE, positions)
    narrow_parts = local_terms(
        query_narrow, key_narrow, value_narrow, decay_narrow, HEAD_NARROW, positions
    )
    local_states = (wide_parts[3], wide_parts[4], narrow_parts[3], narrow_parts[4])
    identity = tuple((jnp.zeros_like(member) for member in local_states))
    carried = prefix_by_axis(local_states, SP, combine, identity)
    mixed_wide = finish(wide_parts, carried[1])
    mixed_narrow = finish(narrow_parts, carried[3])
    rows_dev = length // tp_count
    attention = sent_and_summed(
        (
            jnp.dot(mixed_wide, out_wide, preferred_element_type=jnp.float32)
            + jnp.dot(mixed_narrow, out_narrow, preferred_element_type=jnp.float32)
        ).astype(jnp.bfloat16),
        "tp",
        0,
    )
    hidden_state = residual.astype(jnp.float32) + attention
    scale_row = lax.rsqrt(jnp.mean(hidden_state * hidden_state, axis=-1, keepdims=True) + norm_eps)
    normed = (hidden_state * scale_row * norm_gain).astype(jnp.bfloat16)
    capacity = max(2, 3 * rows_dev * TOP_K // (2 * experts))
    flat_expert = routes.reshape(-1)
    one_hot = (flat_expert[:, None] == jnp.arange(experts, dtype=jnp.int32)[None, :]).astype(
        jnp.int32
    )
    rank_in = jnp.sum((jnp.cumsum(one_hot, axis=0) - one_hot) * one_hot, axis=1)
    slot_index = flat_expert * capacity + rank_in
    source_row = jnp.arange(rows_dev * TOP_K, dtype=jnp.int32) // TOP_K
    slot_table = jnp.zeros((experts * capacity,), jnp.int32).at[slot_index].set(source_row + 1)
    padded = jnp.concatenate([jnp.zeros((1, model_width), jnp.bfloat16), normed], axis=0)
    send_slots = padded[slot_table].reshape(experts, capacity, model_width)
    gate_shard = expert_gate[0]
    up_shard = expert_up[0]
    down_shard = expert_down[0]
    gathered = lax.all_gather(
        core_and_chips(send_slots, ("sp_0", "sp_1"), (1, 0), 0, 0), "tp", axis=0, tiled=True
    )
    flat_rows = gathered.reshape(-1, model_width)
    gate_pre = jnp.dot(flat_rows, gate_shard, preferred_element_type=jnp.float32)
    up_pre = jnp.dot(flat_rows, up_shard, preferred_element_type=jnp.float32)
    hidden = activate(gate_pre, up_pre).astype(jnp.bfloat16)
    partial_value = jnp.dot(hidden, down_shard, preferred_element_type=jnp.float32)
    partial_value = partial_value.reshape(gathered.shape[0], gathered.shape[1], model_width)
    summed = sent_and_summed(
        partial_value.reshape(tp_count, experts, capacity, model_width).astype(jnp.bfloat16),
        "tp",
        0,
    )
    expert_output = summed.reshape(experts, capacity, model_width).astype(jnp.bfloat16)
    returned = lax.all_to_all(expert_output, SP, split_axis=0, concat_axis=0, tiled=True)
    picked = returned.reshape(experts * capacity, model_width)[slot_index].astype(jnp.float32)
    routed = jnp.sum(
        (picked * route_weights.reshape(-1)[:, None]).reshape(rows_dev, TOP_K, model_width), axis=1
    )
    return (hidden_state + routed).astype(jnp.bfloat16)


def solution(mesh):
    torus = Mesh(
        mesh.devices.reshape(mesh.shape["grp"], 16, 2, mesh.shape["tp"]),
        ("grp", "sp_0", "sp_1", "tp"),
    )
    in_specs = (
        P(GRP_SP, "tp"),
        P(GRP_SP, "tp"),
        P(GRP_SP, "tp"),
        P(GRP_SP, "tp"),
        P(GRP_SP, "tp"),
        P(GRP_SP, "tp"),
        P(GRP_SP, "tp"),
        P(GRP_SP, "tp"),
        P(GRP_SP_TP, None),
        P("tp", None),
        P("tp", None),
        P(),
        P(GRP_SP_TP, None),
        P(GRP_SP_TP, None),
        P(SP, None, "tp"),
        P(SP, None, "tp"),
        P(SP, "tp", None),
    )
    out_specs = P(GRP_SP_TP, None)
    return jax.shard_map(body, mesh=torus, in_specs=in_specs, out_specs=out_specs, check_vma=False)
```

profile of v0, /device:TPU:33, one launch (start us, length us, event | category | flops | bytes accessed | tf_op | source)
XLA Modules:
  0.0 619.3 jit_solution(2552972941295234430)
XLA Ops:
  23.0 22.0 %all-gather = bf16[4,128,128]{2,1,0:T(8,128)(2,1)S(1)} all-gather(bf16[2,128,128]{2,1,0:T(8,128)(2,1)S(1)} %convolution_convert_fusion.1), channel_id=2, replica_groups=mesh['grp'=2,'sp_0'=16,'sp_1'=2,'tp'=4] {'sp_1'}, dimensions={0}, use_global_device_ids=true | all-gather | bytes 196608 | tf_op jit(solution)/shard_map/all_gather | solution.py:33
  60.3 32.5 %all_gather.48 = bf16[16,4,64,64]{3,2,1,0:T(8,128)(2,1)S(1)} all-gather(bf16[1,4,64,64]{3,2,1,0:T(8,128)(2,1)S(1)} %fusion.70), channel_id=1, replica_groups=mesh['grp'=2,'sp_0'=16,'sp_1'=2,'tp'=4] {'sp_0'}, dimensions={0}, use_global_device_ids=true | all-gather | bytes 557056 | tf_op jit(solution)/shard_map/all_gather | solution.py:33
  92.8 21.5 %all-gather.5 = bf16[16,1,4]{2,1,0:T(2,128)(2,1)S(1)} all-gather(bf16[1,1,4]{2,1,0:T(2,128)(2,1)S(1)} %get-tuple-element.65), channel_id=1, replica_groups=mesh['grp'=2,'sp_0'=16,'sp_1'=2,'tp'=4] {'sp_0'}, dimensions={0}, use_global_device_ids=true | all-gather | bytes 136 | tf_op jit(solution)/shard_map/all_gather | solution.py:33
  115.0 19.6 %all-gather.3 = bf16[16,1,2]{2,1,0:T(2,128)(2,1)S(1)} all-gather(bf16[1,1,2]{2,1,0:T(2,128)(2,1)} %get-tuple-element.68), channel_id=1, replica_groups=mesh['grp'=2,'sp_0'=16,'sp_1'=2,'tp'=4] {'sp_0'}, dimensions={0}, use_global_device_ids=true | all-gather | bytes 68 | tf_op jit(solution)/shard_map/all_gather | solution.py:33
  136.0 4.1 fusion.31
  152.1 4.7 all-to-all-start
  159.9 12.2 %all-to-all-done = bf16[4,128,2048]{2,1,0:T(8,128)(2,1)} async-done(((bf16[4,128,2048]{2,1,0:T(8,128)(2,1)}), bf16[4,128,2048]{2,1,0:T(8,128)(2,1)}, u32[]{:S(2)}, u32[]{:S(2)}) %all-to-all-start) | async-done | bytes 2097184 | tf_op jit(solution)/shard_map/all_to_all | solution.py:56
  178.7 3.6 reshape_reshape_reshape.3
  184.8 24.9 %all_to_all.25 = bf16[16,2,1,12,2048]{4,0,3,2,1:T(8,128)(2,1)S(1)} all-to-all(bf16[16,2,1,12,2048]{4,0,3,2,1:T(8,128)(2,1)S(1)} %copy.204), channel_id=1, replica_groups=mesh['grp'=2,'sp_0'=16,'sp_1'=2,'tp'=4] {'sp_1'}, dimensions={1} | all-to-all | bytes 3145728 | tf_op jit(solution)/shard_map/all_to_all | solution.py:70
  211.3 72.2 %all_to_all.26 = bf16[16,2,1,12,2048]{4,1,3,2,0:T(2,128)(2,1)S(1)} all-to-all(bf16[16,2,1,12,2048]{4,1,3,2,0:T(2,128)(2,1)S(1)} %copy.205), channel_id=1, replica_groups=mesh['grp'=2,'sp_0'=16,'sp_1'=2,'tp'=4] {'sp_0'}, dimensions={0} | all-to-all | bytes 3145728 | tf_op jit(solution)/shard_map/all_to_all | solution.py:70
  286.1 3.7 reshape_reshape.4
  289.9 72.6 %all-gather.11.cloned.1.call-done = bf16[128,12,2048]{2,0,1:T(8,128)(2,1)} async-done(((bf16[32,12,2048]{2,0,1:T(8,128)(2,1)}), bf16[128,12,2048]{2,0,1:T(8,128)(2,1)}) %all-gather.11.cloned.1.call-update) | async-done | bytes 6291472 | tf_op jit(solution)/shard_map/all_gather | solution.py:211
  362.4 9.7 %copy.207 = bf16[128,12,2048]{2,1,0:T(8,128)(2,1)} copy(bf16[128,12,2048]{2,0,1:T(8,128)(2,1)} %all-gather.11.cloned.1.call-done) | data formatting | bytes 12582912 | tf_op jit(solution)/shard_map/all_gather | solution.py:211
  372.1 10.7 %reshape.746 = bf16[1536,2048]{1,0:T(8,128)(2,1)} reshape(bf16[128,12,2048]{2,1,0:T(8,128)(2,1)} %copy.207) | data formatting | bytes 12582912 | tf_op jit(solution)/shard_map/reshape | solution.py:214
  382.8 6.3 %convolution_minimum_fusion = f32[1536,512]{1,0:T(8,128)S(1)} fusion(bf16[1536,2048]{1,0:T(8,128)(2,1)} %reshape.746, bf16[1,2048,512]{2,1,0:T(8,128)(2,1)} %param.31), kind=kOutput, calls=%fused_computation.13 | convolution fusion | flops 3222011904 | bytes 11534336 | tf_op jit(solution)/shard_map/dot_general | solution.py:215
  389.1 5.0 fusion.7
  394.1 3.6 dot_general.53
  397.7 6.1 convert_bitcast_fusion
  403.8 73.6 %all_to_all.27 = bf16[4,1,32,12,2048]{4,2,3,1,0:T(8,128)(2,1)S(1)} all-to-all(bf16[4,1,32,12,2048]{4,2,3,1,0:T(8,128)(2,1)S(1)} %convert_bitcast_fusion), channel_id=1, replica_groups=mesh['grp'=2,'sp_0'=16,'sp_1'=2,'tp'=4] {'tp'}, dimensions={0} | all-to-all | bytes 12582912 | tf_op jit(solution)/shard_map/all_to_all | solution.py:56
  480.8 14.6 %all-to-all-start.4 = ((bf16[32,12,2048]{2,1,0:T(8,128)(2,1)}), bf16[32,12,2048]{2,1,0:T(8,128)(2,1)}, u32[]{:S(2)}, u32[]{:S(2)}) async-start(bf16[32,12,2048]{2,1,0:T(8,128)(2,1)} %copy.211), calls=%async_computation.4 | async-start | bytes 4194304 | tf_op jit(solution)/shard_map/all_to_all | solution.py:226
  495.6 98.6 %all-to-all-done.4 = bf16[32,12,2048]{2,1,0:T(8,128)(2,1)} async-done(((bf16[32,12,2048]{2,1,0:T(8,128)(2,1)}), bf16[32,12,2048]{2,1,0:T(8,128)(2,1)}, u32[]{:S(2)}, u32[]{:S(2)}) %all-to-all-start.4) | async-done | bytes 1572896 | tf_op jit(solution)/shard_map/all_to_all | solution.py:226
  594.2 3.6 reshape.748
  597.8 4.9 gather_fusion.1
  606.1 4.9 multiply_reduce_fusion
  (167 shorter events, 69.7 us)
Async XLA Ops:
  6.5 391.2 %copy-start = (bf16[1,512,2048]{2,1,0:T(8,128)(2,1)S(1)}, bf16[1,512,2048]{2,1,0:T(8,128)(2,1)}, u32[]{:S(2)}) copy-start(bf16[1,512,2048]{2,1,0:T(8,128)(2,1)} %param.33) | copy-start | bytes 6291460
  6.6 135.7 %all-gather.9.cloned.1.call-start = ((), (), s32[]{:S(2)}) async-start(), calls=%async_computation.5 | async-start | bytes 1114112 | tf_op jit(solution)/shard_map/all_gather | solution.py:33
  22.3 26.0 %copy-start.18 = (f32[512,4]{0,1:T(4,128)S(1)}, f32[512,4]{0,1:T(4,128)}, u32[]{:S(2)}) copy-start(f32[512,4]{0,1:T(4,128)} %param.24) | copy-start | bytes 24580
  22.3 29.9 %copy-start.6 = (bf16[512,256]{1,0:T(8,128)(2,1)S(1)}, bf16[512,256]{1,0:T(8,128)(2,1)}, u32[]{:S(2)}) copy-start(bf16[512,256]{1,0:T(8,128)(2,1)} %param.21) | copy-start | bytes 786436
  22.3 30.0 %copy-start.7 = (bf16[512,256]{1,0:T(8,128)(2,1)S(1)}, bf16[512,256]{1,0:T(8,128)(2,1)}, u32[]{:S(2)}) copy-start(bf16[512,256]{1,0:T(8,128)(2,1)} %param.22) | copy-start | bytes 786436
  22.5 29.6 %copy-start.10 = (bf16[512,2,128]{2,0,1:T(8,128)(2,1)}, bf16[512,2,128]{2,0,1:T(8,128)(2,1)S(1)}, u32[]{:S(2)}) copy-start(bf16[512,2,128]{2,0,1:T(8,128)(2,1)S(1)} %fusion.41) | copy-start | bytes 786436
  54.2 81.8 %copy-start.16 = (f32[1,4,4,128]{3,1,2,0:T(4,128)S(1)}, f32[1,4,4,128]{3,1,2,0:T(4,128)}, u32[]{:S(2)}) copy-start(f32[1,4,4,128]{3,1,2,0:T(4,128)} %copy-done.15) | copy-start | bytes 24580
  56.0 4.3 copy-start.11
  56.0 4.4 copy-start.12
  60.2 75.8 %copy-start.28 = (f32[4]{0:T(128)}, f32[4]{0:T(128)S(1)}, u32[]{:S(2)}) copy-start(f32[4]{0:T(128)S(1)} %get-tuple-element.66) | copy-start | bytes 52
  60.2 75.8 %copy-start.29 = (f32[4]{0:T(128)}, f32[4]{0:T(128)S(1)}, u32[]{:S(2)}) copy-start(f32[4]{0:T(128)S(1)} %get-tuple-element.67) | copy-start | bytes 52
  136.0 4.1 copy-start.14
  142.1 3.2 copy-start.8
  142.1 3.2 copy-start.9
  152.1 4.8 copy-start.19
  152.1 20.0 %all-to-all-start = ((bf16[4,128,2048]{2,1,0:T(8,128)(2,1)}), bf16[4,128,2048]{2,1,0:T(8,128)(2,1)}, u32[]{:S(2)}, u32[]{:S(2)}) async-start(bf16[4,128,2048]{2,1,0:T(8,128)(2,1)} %bitcast.468), calls=%async_computation | async-start | bytes 4194304 | tf_op jit(solution)/shard_map/all_to_all | solution.py:56
  156.8 17.5 %copy-start.4 = (bf16[128,2048]{1,0:T(8,128)(2,1)S(1)}, bf16[128,2048]{1,0:T(8,128)(2,1)}, u32[]{:S(2)}) copy-start(bf16[128,2048]{1,0:T(8,128)(2,1)} %param.25) | copy-start | bytes 1572868
  156.8 205.6 %all-gather.11.cloned.1.call-start = ((), (), s32[]{:S(2)}) async-start(), calls=%async_computation.6 | async-start | bytes 7864320 | tf_op jit(solution)/shard_map/all_gather | solution.py:211
  159.9 15.3 %copy-start.17 = (f32[2048]{0:T(1024)S(1)}, f32[2048]{0:T(1024)}, u32[]{:S(2)}) copy-start(f32[2048]{0:T(1024)} %param.28) | copy-start | bytes 24580
  382.8 6.3 %copy-start.3 = (bf16[1536,2048]{1,0:T(8,128)(2,1)S(1)}, bf16[1536,2048]{1,0:T(8,128)(2,1)}, u32[]{:S(2)}) copy-start(bf16[1536,2048]{1,0:T(8,128)(2,1)} %reshape.746) | copy-start | bytes 18874372
  382.8 6.3 %copy-start.31 = (bf16[1,2048,512]{2,1,0:T(8,128)(2,1)S(1)}, bf16[1,2048,512]{2,1,0:T(8,128)(2,1)}, u32[]{:S(2)}) copy-start(bf16[1,2048,512]{2,1,0:T(8,128)(2,1)} %param.32) | copy-start | bytes 6291460
  480.8 14.6 %copy-start.30 = (f32[128,2]{0,1:T(2,128)S(1)}, f32[128,2]{0,1:T(2,128)}, u32[]{:S(2)}) copy-start(f32[128,2]{0,1:T(2,128)} %param.30) | copy-start | bytes 3076
  480.8 113.3 %all-to-all-start.4 = ((bf16[32,12,2048]{2,1,0:T(8,128)(2,1)}), bf16[32,12,2048]{2,1,0:T(8,128)(2,1)}, u32[]{:S(2)}, u32[]{:S(2)}) async-start(bf16[32,12,2048]{2,1,0:T(8,128)(2,1)} %copy.211), calls=%async_computation.4 | async-start | bytes 4194304 | tf_op jit(solution)/shard_map/all_to_all | solution.py:226
  606.1 4.9 copy-start.2
  (13 other events, 23.4 us)
Sparse Core Ops, SparseCore 0:
  48.3 54.4 all-gather.8
  290.0 72.3 all-gather.10
where the time goes:
time: 626 us; the launch traced here: 619 us
  blocking collectives  272 us (43%)
  waiting for transfers between devices  183 us (29%)
  local copies, waits for them, and re-layouts  72.1 us (12%)
  matrix products  33.7 us (5%)
  other arithmetic  24.1 us (4%)
  starting transfers between devices  19.3 us (3%)
  between operations  14.5 us (2%)
    all_gather x7, blocking collectives, prefix_by_axis(): lax.all_gather(part.astype(kind), axis)  101 us
    all_to_all x1, waiting for transfers between devices, body(): lax.all_to_all(expert_output, SP, split_axis=0, concat_axis=0, tiled=True)  98.6 us
    all_to_all x2, blocking collectives, turned_blocks(): filled = lax.all_to_all(filled, axes[k], k, k, tiled=True)  97.2 us
    all_to_all x1, blocking collectives, sent_and_summed(): lax.all_to_all(pieces, axis, split_axis=0, concat_axis=0, tiled=True)  73.6 us
    all_gather x1, waiting for transfers between devices, body(): lax.all_gather(core_and_chips(send_slots, ('sp_0', 'sp_1'), (1, 0), 0, 0)...  72.6 us
    all_to_all x1, starting transfers between devices, body(): lax.all_to_all(expert_output, SP, split_axis=0, concat_axis=0, tiled=True)  14.6 us
  transfers between devices with their start and end apart: 4, of which 3 were waited for; matrix products, arithmetic and copies ran while one was open for 3% of the time, Pallas kernels for 0%

commit v1 on v0

--- a/solution.py
+++ b/solution.py
@@ -1,6 +1,11 @@
+import functools
+
 import jax
 import jax.numpy as jnp
+import numpy as np
 from jax import lax
+from jax.experimental import pallas as pl
+from jax.experimental.pallas import tpu as pltpu
 from jax.sharding import Mesh
 from jax.sharding import PartitionSpec as P
 
@@ -145,6 +150,440 @@
     gate_clip = jnp.minimum(gate_pre, clamp_limit)
     up_clip = jnp.clip(up_pre, -clamp_limit, clamp_limit)
     return gate_clip * jax.nn.sigmoid(swish_alpha * gate_clip) * (up_clip + 1.0)
+
+
+QUARTERS = 4
+CORES = 2
+MESH = pl.DeviceIdType.MESH
+
+
+def regroup(capacity):
+    rows = 4 * QUARTERS * capacity
+    table = np.zeros((rows, rows), np.float32)
+    for block in range(4):
+        for part in range(QUARTERS):
+            for row in range(capacity):
+                table[
+                    (part * 4 + block) * capacity + row, (block * QUARTERS + part) * capacity + row
+                ] = 1.0
+    return table
+
+
+def experts_kernel(
+    chips,
+    send,
+    perm,
+    perm_back,
+    gate_hbm,
+    up_hbm,
+    down_hbm,
+    out,
+    gbuf,
+    xbuf,
+    hbuf,
+    pbuf,
+    rbuf,
+    sbuf,
+    ret,
+    gate,
+    up,
+    down,
+    load_sem,
+    zs,
+    zr,
+    xs,
+    xr,
+    ys,
+    yr,
+    ds,
+    dr,
+    es,
+    er,
+    rs,
+    rr,
+):
+    z = lax.axis_index("sp_0")
+    c = lax.axis_index("sp_1")
+    x = lax.axis_index("tp")
+    nx = lax.axis_size("tp")
+    me = z * CORES + c
+    half = chips // 2
+    groups = half
+    last = groups - 1
+    right = lax.rem(x + 1, nx)
+    left = lax.rem(x + nx - 1, nx)
+    block_rows = send.shape[1]
+    capacity = block_rows // QUARTERS
+    rows = 4 * capacity
+    width = send.shape[2]
+    half_model = QUARTERS * width // 2
+    hidden_width = gate.shape[1]
+
+    def remote(src, dst, send_sem, recv_sem, to):
+        return pltpu.make_async_remote_copy(
+            src_ref=src,
+            dst_ref=dst,
+            send_sem=send_sem,
+            recv_sem=recv_sem,
+            device_id=to,
+            device_id_type=MESH,
+        )
+
+    def at_z(zt, ct):
+        return {"sp_0": zt, "sp_1": ct}
+
+    def at_x(xt):
+        return {"tp": xt}
+
+    def chip_at(offset):
+        return lax.rem(z + offset + chips, chips)
+
+    barrier = pltpu.get_barrier_semaphore()
+    pl.semaphore_signal(barrier, inc=1, device_id=at_x(right), device_id_type=MESH)
+    pl.semaphore_signal(barrier, inc=1, device_id=at_x(left), device_id_type=MESH)
+    pl.semaphore_signal(barrier, inc=1, device_id=at_z(z, 1 - c), device_id_type=MESH)
+
+    @pl.loop(1, chips)
+    def _(step):
+        for ct in range(CORES):
+            pl.semaphore_signal(
+                barrier, inc=1, device_id=at_z(chip_at(step), ct), device_id_type=MESH
+            )
+
+    loads = [
+        pltpu.make_async_copy(gate_hbm, gate, load_sem.at[0]),
+        pltpu.make_async_copy(up_hbm, up, load_sem.at[1]),
+        pltpu.make_async_copy(down_hbm, down, load_sem.at[2]),
+    ]
+    for load in loads:
+        load.start()
+    pl.semaphore_wait(barrier, 3 + CORES * (chips - 1))
+
+    def partner_out():
+        return remote(
+            send.at[z * CORES + 1 - c], gbuf.at[0, last, c], zs.at[4 * last], zr.at[4 * last],
+            at_z(z, 1 - c),
+        )
+
+    def far_out(ct):
+        zt = chip_at(half)
+        return remote(
+            send.at[zt * CORES + ct],
+            gbuf.at[0, last, 2 + c],
+            zs.at[4 * last + 2 + ct],
+            zr.at[4 * last + 2 + c],
+            at_z(zt, ct),
+        )
+
+    def near_out(d, sign, ct):
+        zt = chip_at(d) if sign == 0 else chip_at(-d)
+        return remote(
+            send.at[zt * CORES + ct],
+            gbuf.at[0, d - 1, 2 * sign + c],
+            zs.at[4 * (d - 1) + 2 * sign + ct],
+            zr.at[4 * (d - 1) + 2 * sign + c],
+            at_z(zt, ct),
+        )
+
+    partner_out().start()
+
+    @pl.loop(1, half)
+    def _(d):
+        for ct in range(CORES):
+            for sign in range(2):
+                near_out(d, sign, ct).start()
+
+    for ct in range(CORES):
+        far_out(ct).start()
+    gbuf[0, last, c] = send[me]
+    for load in loads:
+        load.wait()
+
+    def z_arrived(g, j):
+        return remote(send.at[0], gbuf.at[0, g, j], zs.at[0], zr.at[4 * g + j], at_z(z, 1 - c))
+
+    def spread(side, g):
+        return remote(
+            gbuf.at[0, g],
+            gbuf.at[1 + side, g],
+            xs.at[side, g],
+            xr.at[side, g],
+            at_x(right if side == 0 else left),
+        )
+
+    def relay(side, g):
+        return remote(
+            gbuf.at[1 + side, g, pl.ds(2 * side, 2)],
+            gbuf.at[3, g, pl.ds(2 * side, 2)],
+            ys.at[side, g],
+            yr.at[side, g],
+            at_x(right if side == 0 else left),
+        )
+
+    def stage_a(g):
+        @pl.when(g < last)
+        def _():
+            for j in range(4):
+                z_arrived(g, j).wait_recv()
+
+        @pl.when(g == last)
+        def _():
+            for j in (0, 2, 3):
+                z_arrived(g, j).wait_recv()
+
+        for side in range(2):
+            spread(side, g).start()
+
+    def stage_b(g):
+        for side in range(2):
+            spread(side, g).wait_recv()
+            relay(side, g).start()
+
+    def far_half(side, g):
+        return remote(
+            pbuf.at[g, 3, side],
+            rbuf.at[side, g],
+            ds.at[side, g],
+            dr.at[side, g],
+            at_x(right if side == 0 else left),
+        )
+
+    def plain_half(side, g):
+        return remote(
+            pbuf.at[g, 2 - side, 1 - side],
+            sbuf.at[side, 1 - side, g],
+            es.at[side, 0, g],
+            er.at[side, 0, g],
+            at_x(right if side == 0 else left),
+        )
+
+    def added_half(side, g):
+        return remote(
+            pbuf.at[g, 2 - side, side],
+            sbuf.at[side, side, g],
+            es.at[side, 1, g],
+            er.at[side, 1, g],
+            at_x(right if side == 0 else left),
+        )
+
+    def stage_c(g):
+        for side in range(2):
+            relay(side, g).wait_recv()
+        for part in range(4):
+            block = gbuf[part, g].reshape(4 * block_rows, width)
+            turned = jnp.dot(perm[...], block, preferred_element_type=jnp.float32).astype(
+                jnp.bfloat16
+            )
+            for q in range(QUARTERS):
+                xbuf[pl.ds(part * rows, rows), pl.ds(q * width, width)] = turned[
+                    q * rows : (q + 1) * rows
+                ]
+        step = min(256, hidden_width)
+
+        @pl.loop(0, hidden_width // step)
+        def _(n):
+            cols = pl.ds(pl.multiple_of(n * step, step), step)
+            gate_pre = jnp.dot(xbuf[...], gate[:, cols], preferred_element_type=jnp.float32)
+            up_pre = jnp.dot(xbuf[...], up[:, cols], preferred_element_type=jnp.float32)
+            hbuf[:, cols] = activate(gate_pre, up_pre).astype(jnp.bfloat16)
+
+        out_step = min(512, half_model)
+
+        @pl.loop(0, half_model // out_step)
+        def _(n):
+            for side in range(2):
+                cols = pl.ds(
+                    pl.multiple_of(side * half_model + n * out_step, out_step), out_step
+                )
+                here = pl.ds(pl.multiple_of(n * out_step, out_step), out_step)
+                part_sum = jnp.dot(
+                    hbuf[...], down[:, cols], preferred_element_type=jnp.float32
+                ).astype(jnp.bfloat16)
+                for part in range(4):
+                    pbuf[g, part, side, :, here] = part_sum[part * rows : (part + 1) * rows]
+
+        for side in range(2):
+            far_half(side, g).start()
+        for side in range(2):
+            plain_half(side, g).start()
+
+    def stage_e(g):
+        for side in range(2):
+            far_half(side, g).wait_recv()
+            pbuf[g, 2 - side, side] = (
+                pbuf[g, 2 - side, side].astype(jnp.float32) + rbuf[side, g].astype(jnp.float32)
+            ).astype(jnp.bfloat16)
+            added_half(side, g).start()
+
+    def stage_f(g):
+        for side in range(2):
+            plain_half(side, g).wait_recv()
+            added_half(side, g).wait_recv()
+        quarters = []
+        for h in range(2):
+            total = (
+                pbuf[g, 0, h].astype(jnp.float32)
+                + sbuf[0, h, g].astype(jnp.float32)
+                + sbuf[1, h, g].astype(jnp.float32)
+            ).astype(jnp.bfloat16)
+            quarters += [total[:, :width], total[:, width:]]
+        stacked = jnp.concatenate(quarters, axis=0)
+        ret[g] = (
+            jnp.dot(perm_back[...], stacked, preferred_element_type=jnp.float32)
+            .astype(jnp.bfloat16)
+            .reshape(4, block_rows, width)
+        )
+
+    def near_back(g, sign, cs):
+        zt = chip_at(-g - 1) if sign == 0 else chip_at(g + 1)
+        return remote(
+            ret.at[g, 2 * sign + cs],
+            out.at[me],
+            rs.at[4 * g + 2 * sign + cs],
+            rr.at[4 * g + 2 * sign + c],
+            at_z(zt, cs),
+        )
+
+    def far_back(cs):
+        return remote(
+            ret.at[last, 2 + cs],
+            out.at[me],
+            rs.at[4 * last + 2 + cs],
+            rr.at[4 * last + 2 + c],
+            at_z(chip_at(half), cs),
+        )
+
+    def partner_back():
+        return remote(
+            ret.at[last, 1 - c], out.at[me], rs.at[4 * last], rr.at[4 * last], at_z(z, 1 - c)
+        )
+
+    def stage_h(g):
+        @pl.when(g < last)
+        def _():
+            for cs in range(CORES):
+                for sign in range(2):
+                    near_back(g, sign, cs).start()
+
+        @pl.when(g == last)
+        def _():
+            for cs in range(CORES):
+                far_back(cs).start()
+            partner_back().start()
+            out[me] = ret[last, c]
+
+    @pl.loop(0, groups + 4)
+    def _(i):
+        @pl.when(i >= 4)
+        def _():
+            stage_f(i - 4)
+
+        @pl.when(i >= groups)
+        def _():
+            stage_h(i - 4)
+
+        @pl.when((i >= 3) & (i < groups + 3))
+        def _():
+            stage_e(i - 3)
+
+        @pl.when((i >= 2) & (i < groups + 2))
+        def _():
+            stage_c(i - 2)
+
+        @pl.when((i >= 1) & (i < groups + 1))
+        def _():
+            stage_b(i - 1)
+
+        @pl.when(i < groups)
+        def _():
+            stage_a(i)
+
+        @pl.when(i == last)
+        def _():
+            @pl.loop(0, groups - 4)
+            def _(g):
+                stage_h(g)
+
+    partner_out().wait_send()
+    partner_back().wait_send()
+    partner_back().wait_recv()
+    for ct in range(CORES):
+        far_out(ct).wait_send()
+        far_back(ct).wait_send()
+
+    def back_arrived(g, j):
+        return remote(ret.at[0, 0], out.at[0], rs.at[0], rr.at[4 * g + j], at_z(z, 1 - c))
+
+    for j in (2, 3):
+        back_arrived(last, j).wait_recv()
+
+    @pl.loop(0, last)
+    def _(g):
+        for sign in range(2):
+            for ct in range(CORES):
+                near_out(g + 1, sign, ct).wait_send()
+                near_back(g, sign, ct).wait_send()
+        for j in range(4):
+            back_arrived(g, j).wait_recv()
+
+    @pl.loop(0, groups)
+    def _(g):
+        for side in range(2):
+            spread(side, g).wait_send()
+            relay(side, g).wait_send()
+            far_half(side, g).wait_send()
+            plain_half(side, g).wait_send()
+            added_half(side, g).wait_send()
+
+
+def experts_stage(send, gate, up, down):
+    experts, block_rows, width = send.shape
+    chips = lax.axis_size("sp_0")
+    groups = chips // 2
+    capacity = block_rows // QUARTERS
+    rows = 4 * capacity
+    model_width = QUARTERS * width
+    hidden_width = gate.shape[1]
+    table = regroup(capacity)
+    vmem = pl.BlockSpec(memory_space=pltpu.VMEM)
+    hbm = pl.BlockSpec(memory_space=pl.ANY)
+    bf16 = jnp.bfloat16
+    dma = pltpu.SemaphoreType.DMA
+    return pl.pallas_call(
+        functools.partial(experts_kernel, chips),
+        out_shape=jax.ShapeDtypeStruct(send.shape, bf16),
+        in_specs=[vmem, vmem, vmem, hbm, hbm, hbm],
+        out_specs=vmem,
+        scratch_shapes=[
+            pltpu.VMEM((4, groups, 4, block_rows, width), bf16),
+            pltpu.VMEM((4 * rows, model_width), bf16),
+            pltpu.VMEM((4 * rows, hidden_width), bf16),
+            pltpu.VMEM((groups, 4, 2, rows, model_width // 2), bf16),
+            pltpu.VMEM((2, groups, rows, model_width // 2), bf16),
+            pltpu.VMEM((2, 2, groups, rows, model_width // 2), bf16),
+            pltpu.VMEM((groups, 4, block_rows, width), bf16),
+            pltpu.VMEM(gate.shape, bf16),
+            pltpu.VMEM(up.shape, bf16),
+            pltpu.VMEM(down.shape, bf16),
+            dma((3,)),
+            dma((4 * groups,)),
+            dma((4 * groups,)),
+            dma((2, groups)),
+            dma((2, groups)),
+            dma((2, groups)),
+            dma((2, groups)),
+            dma((2, groups)),
+            dma((2, groups)),
+            dma((2, 2, groups)),
+            dma((2, 2, groups)),
+            dma((4 * groups,)),
+            dma((4 * groups,)),
+        ],
+        compiler_params=pltpu.CompilerParams(
+            collective_id=0, has_side_effects=True, vmem_limit_bytes=48 * 1024 * 1024
+        ),
+        name="experts_stage",
+    )(send, jnp.asarray(table, bf16), jnp.asarray(table.T, bf16), gate, up, down)
 
 
 def body(
@@ -200,33 +639,32 @@
         jnp.int32
     )
     rank_in = jnp.sum((jnp.cumsum(one_hot, axis=0) - one_hot) * one_hot, axis=1)
-    slot_index = flat_expert * capacity + rank_in
-    source_row = jnp.arange(rows_dev * TOP_K, dtype=jnp.int32) // TOP_K
-    slot_table = jnp.zeros((experts * capacity,), jnp.int32).at[slot_index].set(source_row + 1)
-    padded = jnp.concatenate([jnp.zeros((1, model_width), jnp.bfloat16), normed], axis=0)
-    send_slots = padded[slot_table].reshape(experts, capacity, model_width)
-    gate_shard = expert_gate[0]
-    up_shard = expert_up[0]
-    down_shard = expert_down[0]
-    gathered = lax.all_gather(
-        core_and_chips(send_slots, ("sp_0", "sp_1"), (1, 0), 0, 0), "tp", axis=0, tiled=True
-    )
-    flat_rows = gathered.reshape(-1, model_width)
-    gate_pre = jnp.dot(flat_rows, gate_shard, preferred_element_type=jnp.float32)
-    up_pre = jnp.dot(flat_rows, up_shard, preferred_element_type=jnp.float32)
-    hidden = activate(gate_pre, up_pre).astype(jnp.bfloat16)
-    partial_value = jnp.dot(hidden, down_shard, preferred_element_type=jnp.float32)
-    partial_value = partial_value.reshape(gathered.shape[0], gathered.shape[1], model_width)
-    summed = sent_and_summed(
-        partial_value.reshape(tp_count, experts, capacity, model_width).astype(jnp.bfloat16),
-        "tp",
-        0,
-    )
-    expert_output = summed.reshape(experts, capacity, model_width).astype(jnp.bfloat16)
-    returned = lax.all_to_all(expert_output, SP, split_axis=0, concat_axis=0, tiled=True)
-    picked = returned.reshape(experts * capacity, model_width)[slot_index].astype(jnp.float32)
-    routed = jnp.sum(
-        (picked * route_weights.reshape(-1)[:, None]).reshape(rows_dev, TOP_K, model_width), axis=1
+    place = (flat_expert * (QUARTERS * capacity) + rank_in).reshape(rows_dev, TOP_K)
+    width = model_width // QUARTERS
+    places = (
+        place[None] + (jnp.arange(QUARTERS, dtype=jnp.int32) * capacity)[:, None, None]
+    ).reshape(QUARTERS * rows_dev, TOP_K)
+    slots = jnp.arange(experts * QUARTERS * capacity, dtype=jnp.int32)
+    chosen = (slots[:, None] == places[None, :, 0]) | (slots[:, None] == places[None, :, 1])
+    parted = jnp.concatenate(
+        [normed[:, q * width : (q + 1) * width] for q in range(QUARTERS)], axis=0
+    )
+    send = jnp.dot(
+        chosen.astype(jnp.bfloat16), parted, preferred_element_type=jnp.float32
+    ).astype(jnp.bfloat16)
+    back = experts_stage(
+        send.reshape(experts, QUARTERS * capacity, width),
+        expert_gate[0],
+        expert_up[0],
+        expert_down[0],
+    ).reshape(experts * QUARTERS * capacity, width)
+    routed = jnp.zeros((QUARTERS * rows_dev, width), jnp.float32)
+    for k in range(TOP_K):
+        picks = (places[:, k][:, None] == slots[None, :]).astype(jnp.bfloat16)
+        picked = jnp.dot(picks, back, preferred_element_type=jnp.float32)
+        routed = routed + picked * jnp.tile(route_weights[:, k], QUARTERS)[:, None]
+    routed = jnp.concatenate(
+        [routed[q * rows_dev : (q + 1) * rows_dev] for q in range(QUARTERS)], axis=1
     )
     return (hidden_state + routed).astype(jnp.bfloat16)
 

time: 626 us -> 357 us (0.57)
  Pallas kernels: 0 us -> 177 us
  blocking collectives: 272 us -> 99.7 us
  waiting for transfers between devices: 183 us -> 13 us
  local copies, waits for them, and re-layouts: 72.1 us -> 13.6 us
  matrix products: 33.7 us -> 18.9 us
  starting transfers between devices: 19.3 us -> 5.2 us
  other arithmetic: 24.1 us -> 14 us
    pallas_call x0 -> x1, Pallas kernels: none -> 177 us  [experts_stage(): pl.pallas_call(functools.partial(experts_kernel, chips), out_shape=jax.Sh...]
    all_to_all x3 -> x0, blocking collectives: 171 us -> none  [the longest x2 97.2 us: turned_blocks(): filled = lax.all_to_all(filled, axes[k], k, k, tiled=True)]
    all_to_all x1 -> x0, waiting for transfers between devices: 98.6 us -> none  [body(): lax.all_to_all(expert_output, SP, split_axis=0, concat_axis=0, tiled=True)]
    all_gather x1 -> x0, waiting for transfers between devices: 72.6 us -> none  [body(): lax.all_gather(core_and_chips(send_slots, ('sp_0', 'sp_1'), (1, 0), 0, 0)...]
    all_to_all x1 -> x0, starting transfers between devices: 14.6 us -> none  [body(): lax.all_to_all(expert_output, SP, split_axis=0, concat_axis=0, tiled=True)]
    reshape x3 -> x1, local copies, waits for them, and re-layouts: 15.2 us -> 0.8 us  [the longest x1 10.7 us: body(): flat_rows = gathered.reshape(-1, model_width)]
    dot_general x3, matrix products: 17.4 us -> 3.4 us  [the longest x2 2.35 us: body(): picked = jnp.dot(picks, back, preferred_element_type=jnp.float32)]
    another operation x7 -> x5, local copies, waits for them, and re-layouts: 10.1 us -> 0.36 us  [the longest x2 6.06 us: turned_blocks(): filled = pieces.reshape(*(lax.axis_size(a) for a in axes), *inside)]
  transfers between devices with their start and end apart: 4 -> 2, of which waited for: 3 -> 1; matrix products, arithmetic and copies ran while one was open for 3% -> 6% of each run, Pallas kernels for 0% -> 0%
where the time goes in v1:
time: 357 us; the launch traced here: 356 us
  Pallas kernels  177 us (50%)
  blocking collectives  99.7 us (28%)
  matrix products  18.9 us (5%)
  other arithmetic  14 us (4%)
  between operations  14 us (4%)
  local copies, waits for them, and re-layouts  13.6 us (4%)
  waiting for transfers between devices  13 us (4%)
  starting transfers between devices  5.2 us (1%)
    pallas_call x1, Pallas kernels, experts_stage(): pl.pallas_call(functools.partial(experts_kernel, chips), out_shape=jax.Sh...  177 us
    all_gather x7, blocking collectives, prefix_by_axis(): lax.all_gather(part.astype(kind), axis)  99.7 us
    all_to_all x1, waiting for transfers between devices, sent_and_summed(): lax.all_to_all(pieces, axis, split_axis=0, concat_axis=0, tiled=True)  13 us
  transfers between devices with their start and end apart: 2, of which 1 were waited for; matrix products, arithmetic and copies ran while one was open for 6% of the time, Pallas kernels for 0%

profile of v1, /device:TPU:33, one launch (start us, length us, event | category | flops | bytes accessed | tf_op | source)
XLA Modules:
  0.0 355.8 jit_solution(57360070514868123)
XLA Ops:
  8.8 1.1 copy.117
  14.4 22.0 %all-gather = bf16[4,128,128]{2,1,0:T(8,128)(2,1)S(1)} all-gather(bf16[2,128,128]{2,1,0:T(8,128)(2,1)S(1)} %convolution_convert_fusion.1), channel_id=2, replica_groups=mesh['grp'=2,'sp_0'=16,'sp_1'=2,'tp'=4] {'sp_1'}, dimensions={0}, use_global_device_ids=true | all-gather | bytes 196608 | tf_op jit(solution)/shard_map/all_gather | solution.py:38
  36.4 1.8 all-gather.2
  40.3 1.2 reduce-window.24
  47.3 1.3 convolution_convert_fusion
  48.6 2.0 all-gather.1
  50.6 1.9 all-gather.4
  52.6 31.4 %all_gather.45 = bf16[16,4,64,64]{3,2,1,0:T(8,128)(2,1)S(1)} all-gather(bf16[1,4,64,64]{3,2,1,0:T(8,128)(2,1)S(1)} %fusion.86), channel_id=1, replica_groups=mesh['grp'=2,'sp_0'=16,'sp_1'=2,'tp'=4] {'sp_0'}, dimensions={0}, use_global_device_ids=true | all-gather | bytes 557056 | tf_op jit(solution)/shard_map/all_gather | solution.py:38
  84.0 20.3 %all-gather.5 = bf16[16,1,4]{2,1,0:T(2,128)(2,1)S(1)} all-gather(bf16[1,1,4]{2,1,0:T(2,128)(2,1)S(1)} %get-tuple-element.77), channel_id=1, replica_groups=mesh['grp'=2,'sp_0'=16,'sp_1'=2,'tp'=4] {'sp_0'}, dimensions={0}, use_global_device_ids=true | all-gather | bytes 136 | tf_op jit(solution)/shard_map/all_gather | solution.py:38
  105.0 20.3 %all-gather.3 = bf16[16,1,2]{2,1,0:T(2,128)(2,1)S(1)} all-gather(bf16[1,1,2]{2,1,0:T(2,128)(2,1)S(1)} %copy-done.29), channel_id=1, replica_groups=mesh['grp'=2,'sp_0'=16,'sp_1'=2,'tp'=4] {'sp_0'}, dimensions={0}, use_global_device_ids=true | all-gather | bytes 68 | tf_op jit(solution)/shard_map/all_gather | solution.py:38
  127.3 3.9 %fusion.39 = f32[512,4,64]{0,2,1:T(8,128)} fusion(bf16[512,4,64]{0,2,1:T(8,128)(2,1)} %bitcast.482, f32[4,512]{1,0:T(4,128)S(1)} %bitcast.485, pred[512,512]{1,0:T(8,128)(4,1)} %iota_compare_fusion.13, bf16[512,4,32]{0,2,1:T(8,128)(2,1)S(1)} %get-tuple-element.27, bf16[512,4,32]{0,2,1:T(8,128)(2,1)} %get-tuple-element.28, f32[512,4,32]{0,2,1:T(8,128)} %copy-done.8, ...), kind=kOutput, calls=%fused_computation.36 | convolution fusion | flops 272498688 | bytes 1843200 | tf_op jit(solution)/shard_map/hts,she->the/dot_general | solution.py:126
  131.2 1.9 fusion.344
  133.4 2.8 fusion.42
  136.3 2.2 fusion.343
  139.9 2.1 add_convert_fusion
  142.0 5.2 %all-to-all-start = ((bf16[4,128,2048]{2,1,0:T(8,128)(2,1)}), bf16[4,128,2048]{2,1,0:T(8,128)(2,1)S(1)}, u32[]{:S(2)}, u32[]{:S(2)}) async-start(bf16[4,128,2048]{2,1,0:T(8,128)(2,1)} %bitcast.472), calls=%async_computation | async-start | bytes 4194304 | tf_op jit(solution)/shard_map/all_to_all | solution.py:61
  147.2 2.0 copy.116
  149.6 13.0 %all-to-all-done = bf16[4,128,2048]{2,1,0:T(8,128)(2,1)S(1)} async-done(((bf16[4,128,2048]{2,1,0:T(8,128)(2,1)}), bf16[4,128,2048]{2,1,0:T(8,128)(2,1)S(1)}, u32[]{:S(2)}, u32[]{:S(2)}) %all-to-all-start) | async-done | bytes 2097184 | tf_op jit(solution)/shard_map/all_to_all | solution.py:61
  162.6 1.4 convert_reduce_fusion
  164.0 1.6 copy.131
  166.3 1.1 fusion.10
  167.9 177.4 %experts_stage.1 = bf16[32,48,512]{2,1,0:T(8,128)(2,1)S(1)} custom-call(bf16[32,48,512]{2,1,0:T(8,128)(2,1)S(1)} %bitcast.471, bf16[192,192]{1,0:T(8,128)(2,1)S(1)} %copy-done.2, bf16[192,192]{1,0:T(8,128)(2,1)S(1)} %copy-done.2, bf16[2048,512]{1,0:T(8,128)(2,1)S(1)} %bitcast.468, bf16[2048,512]{1,0:T(8,128)(2,1)} %bitcast.477, bf16[512,2048]{1,0:T(8,128)(2,1)} %bitcast.478), custom_call_target="tpu_custom_call" | custom-call | tf_op jit(solution)/shard_map/experts_stage/pallas_call | solution.py:552
  345.3 1.2 fusion.30
  346.5 1.2 fusion.32
  (149 shorter events, 21.5 us)
Async XLA Ops:
  6.5 132.1 %copy-start = (bf16[256,2048]{1,0:T(8,128)(2,1)S(1)}, bf16[256,2048]{1,0:T(8,128)(2,1)}, u32[]{:S(2)}) copy-start(bf16[256,2048]{1,0:T(8,128)(2,1)} %param.28) | copy-start | bytes 3145732
  6.6 3.8 %copy-start.9 = (bf16[512,256]{1,0:T(8,128)(2,1)S(1)}, bf16[512,256]{1,0:T(8,128)(2,1)}, u32[]{:S(2)}) copy-start(bf16[512,256]{1,0:T(8,128)(2,1)} %param.20) | copy-start | bytes 786436
  6.6 126.8 %all-gather.8.cloned.1.call-start = ((), (), s32[]{:S(2)}) async-start(), calls=%async_computation.1 | async-start | bytes 1114112 | tf_op jit(solution)/shard_map/all_gather | solution.py:38
  13.6 26.7 %copy-start.13 = (f32[512,4]{0,1:T(4,128)S(1)}, f32[512,4]{0,1:T(4,128)}, u32[]{:S(2)}) copy-start(f32[512,4]{0,1:T(4,128)} %param.26) | copy-start | bytes 24580
  13.6 29.3 %copy-start.14 = (s32[128,2]{0,1:T(2,128)S(1)}, s32[128,2]{0,1:T(2,128)}, u32[]{:S(2)}) copy-start(s32[128,2]{0,1:T(2,128)} %param.31) | copy-start | bytes 3076
  13.6 31.1 %copy-start.5 = (bf16[512,256]{1,0:T(8,128)(2,1)S(1)}, bf16[512,256]{1,0:T(8,128)(2,1)}, u32[]{:S(2)}) copy-start(bf16[512,256]{1,0:T(8,128)(2,1)} %param.23) | copy-start | bytes 786436
  13.6 31.3 %copy-start.6 = (bf16[512,256]{1,0:T(8,128)(2,1)S(1)}, bf16[512,256]{1,0:T(8,128)(2,1)}, u32[]{:S(2)}) copy-start(bf16[512,256]{1,0:T(8,128)(2,1)} %param.24) | copy-start | bytes 786436
  13.6 31.4 %copy-start.10 = (bf16[512,256]{1,0:T(8,128)(2,1)S(1)}, bf16[512,256]{1,0:T(8,128)(2,1)}, u32[]{:S(2)}) copy-start(bf16[512,256]{1,0:T(8,128)(2,1)} %param.25) | copy-start | bytes 786436
  38.2 5.5 %copy-start.22 = (bf16[2,1,2]{2,1,0:T(2,128)(2,1)}, bf16[2,1,2]{2,1,0:T(2,128)(2,1)S(1)}, u32[]{:S(2)}) copy-start(bf16[2,1,2]{2,1,0:T(2,128)(2,1)S(1)} %all-gather.2) | copy-start | bytes 28
  38.7 5.0 %copy-start.24 = (f32[2]{0:T(128)}, f32[2]{0:T(128)S(1)}, u32[]{:S(2)}) copy-start(f32[2]{0:T(128)S(1)} %get-tuple-element.81) | copy-start | bytes 28
  38.7 5.0 %copy-start.26 = (f32[2]{0:T(128)}, f32[2]{0:T(128)S(1)}, u32[]{:S(2)}) copy-start(f32[2]{0:T(128)S(1)} %get-tuple-element.82) | copy-start | bytes 28
  47.3 5.2 %copy-start.8 = (f32[512,4,32]{0,2,1:T(8,128)}, f32[512,4,32]{0,2,1:T(8,128)S(1)}, u32[]{:S(2)}) copy-start(f32[512,4,32]{0,2,1:T(8,128)S(1)} %get-tuple-element.14) | copy-start | bytes 786436
  47.3 57.7 %copy-start.29 = (bf16[1,1,2]{2,1,0:T(2,128)(2,1)S(1)}, bf16[1,1,2]{2,1,0:T(2,128)(2,1)}, u32[]{:S(2)}) copy-start(bf16[1,1,2]{2,1,0:T(2,128)(2,1)} %get-tuple-element.80) | copy-start | bytes 16
  47.3 78.0 %copy-start.18 = (s32[2,128]{1,0:T(2,128)S(1)}, s32[2,128]{1,0:T(2,128)}, u32[]{:S(2)}) copy-start(s32[2,128]{1,0:T(2,128)} %eq.85) | copy-start | bytes 3076
  47.3 79.4 %copy-start.17 = (s32[256]{0:T(256)S(1)}, s32[256]{0:T(256)}, u32[]{:S(2)}) copy-start(s32[256]{0:T(256)} %eq.81) | copy-start | bytes 3076
  52.4 52.5 %copy-start.27 = (f32[4]{0:T(128)}, f32[4]{0:T(128)S(1)}, u32[]{:S(2)}) copy-start(f32[4]{0:T(128)S(1)} %get-tuple-element.78) | copy-start | bytes 52
  52.5 52.5 %copy-start.28 = (f32[4]{0:T(128)}, f32[4]{0:T(128)S(1)}, u32[]{:S(2)}) copy-start(f32[4]{0:T(128)S(1)} %get-tuple-element.79) | copy-start | bytes 52
  133.3 3.0 copy-start.11
  133.3 3.0 copy-start.21
  133.3 3.0 copy-start.32
  142.0 7.3 %copy-start.16 = (s32[256]{0:T(256)S(1)}, s32[256]{0:T(256)}, u32[]{:S(2)}) copy-start(s32[256]{0:T(256)} %fusion.237) | copy-start | bytes 3076
  142.0 7.5 %copy-start.30 = (f32[128,2]{0,1:T(2,128)S(1)}, f32[128,2]{0,1:T(2,128)}, u32[]{:S(2)}) copy-start(f32[128,2]{0,1:T(2,128)} %param.32) | copy-start | bytes 3076
  142.0 7.5 %copy-start.15 = (s32[128,2]{0,1:T(2,128)S(1)}, s32[128,2]{0,1:T(2,128)}, u32[]{:S(2)}) copy-start(s32[128,2]{0,1:T(2,128)} %param.31) | copy-start | bytes 3076
  142.0 20.6 %all-to-all-start = ((bf16[4,128,2048]{2,1,0:T(8,128)(2,1)}), bf16[4,128,2048]{2,1,0:T(8,128)(2,1)S(1)}, u32[]{:S(2)}, u32[]{:S(2)}) async-start(bf16[4,128,2048]{2,1,0:T(8,128)(2,1)} %bitcast.472), calls=%async_computation | async-start | bytes 4194304 | tf_op jit(solution)/shard_map/all_to_all | solution.py:61
  (11 other events, 19.9 us)
Sparse Core Ops, SparseCore 0:
  39.6 54.5 all-gather.7

commit v2 on v1

--- a/solution.py
+++ b/solution.py
@@ -21,129 +21,6 @@
 clamp_limit = 7.0
 swish_alpha = 1.702
 rotary_base = 10000.0
-
-
-def filled_with(value, identity):
-    return jax.tree.map(
-        lambda a, e: jnp.broadcast_to(jnp.asarray(e, a.dtype), a.shape), value, identity
-    )
-
-
-def prefix_by_axis(value, axes, combine, identity):
-    before = start = filled_with(value, identity)
-    total = value
-    for axis in reversed(axes):
-        length, mine = (lax.axis_size(axis), lax.axis_index(axis))
-        pieces = jax.tree.map(
-            lambda part, kind: lax.all_gather(part.astype(kind), axis),
-            total,
-            jax.tree.map(lambda a: jnp.bfloat16 if a.dtype == jnp.float32 else a.dtype, value),
-        )
-        inside, total = (start, start)
-        for k in range(length):
-            passed = k < mine
-            total = combine(
-                total, jax.tree.map(lambda part, own: part[k].astype(own.dtype), pieces, value)
-            )
-            inside = jax.tree.map(lambda new, old: jnp.where(passed, new, old), total, inside)
-        before = combine(inside, before)
-    return before
-
-
-def cut_along(value, dim, length):
-    lengths = value.shape
-    pieces = value.reshape(*lengths[:dim], length, lengths[dim] // length, *lengths[dim + 1 :])
-    return jnp.moveaxis(pieces, dim, 0)
-
-
-def sent_and_summed(value, axis, dim):
-    pieces = cut_along(value, dim, lax.axis_size(axis))
-    arrived = lax.all_to_all(pieces, axis, split_axis=0, concat_axis=0, tiled=True)
-    return arrived.astype(jnp.float32).sum(axis=0)
-
-
-def laid_out(pieces, dim):
-    pieces = jnp.moveaxis(pieces, 0, dim)
-    lengths = pieces.shape
-    return pieces.reshape(*lengths[:dim], lengths[dim] * lengths[dim + 1], *lengths[dim + 2 :])
-
-
-def turned_blocks(pieces, axes, order):
-    inside = pieces.shape[1:]
-    filled = pieces.reshape(*(lax.axis_size(a) for a in axes), *inside)
-    for k in order:
-        filled = lax.all_to_all(filled, axes[k], k, k, tiled=True)
-    return filled.reshape(-1, *inside)
-
-
-def core_and_chips(value, groups, order, split_dim, concat_dim):
-    length = lax.axis_size(groups[0]) * lax.axis_size(groups[1])
-    pieces = cut_along(value, split_dim, length)
-    return laid_out(turned_blocks(pieces, groups, order), concat_dim)
-
-
-def rotate(values, positions):
-    half_width = values.shape[-1] // 2
-    inverse = rotary_base ** (-jnp.arange(half_width, dtype=jnp.float32) / half_width)
-    angles = positions[:, None] * inverse[None, :]
-    cosine = jnp.cos(angles)[:, None, :]
-    sine_part = jnp.sin(angles)[:, None, :]
-    lower_half = values[..., :half_width]
-    upper_half = values[..., half_width:]
-    return jnp.concatenate(
-        [
-            lower_half * cosine - upper_half * sine_part,
-            lower_half * sine_part + upper_half * cosine,
-        ],
-        axis=-1,
-    )
-
-
-def group_norm(output_heads):
-    center = jnp.mean(output_heads, axis=-1, keepdims=True)
-    spread = jnp.mean(jnp.square(output_heads - center), axis=-1, keepdims=True)
-    return (output_heads - center) * lax.rsqrt(spread + norm_eps)
-
-
-def local_terms(query_in, key_in, value_in, log_decay, head_width, positions):
-    length = query_in.shape[0]
-    attention_group_count = query_in.shape[1] // head_width
-    query_heads = query_in.astype(jnp.float32).reshape(length, attention_group_count, head_width)
-    key_heads = key_in.astype(jnp.float32).reshape(length, attention_group_count, head_width)
-    query_f = rotate(query_heads, positions).astype(jnp.bfloat16).astype(jnp.float32)
-    key_f = (
-        (rotate(key_heads, positions) * head_width ** (-0.5))
-        .astype(jnp.bfloat16)
-        .astype(jnp.float32)
-    )
-    value_f = value_in.reshape(length, attention_group_count, head_width).astype(jnp.float32)
-    cumulative = jnp.cumsum(log_decay, axis=0)
-    steps_in = jnp.arange(length, dtype=jnp.int32)
-    causal = steps_in[:, None] >= steps_in[None, :]
-    gaps = cumulative.T[:, :, None] - cumulative.T[:, None, :]
-    decay_grid = jnp.exp(jnp.where(causal[None], gaps, -jnp.inf))
-    scores = jnp.einsum("thd,shd->hts", query_f, key_f) * decay_grid
-    inner_part = jnp.einsum("hts,she->the", scores, value_f)
-    total_log = cumulative[-1]
-    weighted = key_f * jnp.exp(total_log[None, :] - cumulative)[:, :, None]
-    state_local = jnp.einsum("shd,she->hde", weighted, value_f)
-    return (query_f, cumulative, inner_part, total_log, state_local)
-
-
-def finish(parts, state_in):
-    query_f, cumulative, inner_part = (parts[0], parts[1], parts[2])
-    carried_part = jnp.exp(cumulative)[:, :, None] * jnp.einsum("thd,hde->the", query_f, state_in)
-    normed_heads = group_norm(inner_part + carried_part)
-    return normed_heads.reshape(normed_heads.shape[0], -1).astype(jnp.bfloat16)
-
-
-def combine(earlier, later):
-    return (
-        earlier[0] + later[0],
-        jnp.exp(later[0])[:, None, None] * earlier[1] + later[1],
-        earlier[2] + later[2],
-        jnp.exp(later[2])[:, None, None] * earlier[3] + later[3],
-    )
 
 
 def activate(gate_pre, up_pre):
@@ -586,6 +463,476 @@
     )(send, jnp.asarray(table, bf16), jnp.asarray(table.T, bf16), gate, up, down)
 
 
+def in_three(value):
+    first = value.astype(jnp.bfloat16)
+    rest = value - first.astype(jnp.float32)
+    second = rest.astype(jnp.bfloat16)
+    third = (rest - second.astype(jnp.float32)).astype(jnp.bfloat16)
+    return (first, second, third)
+
+
+def lanes_of(shape):
+    return lax.broadcasted_iota(jnp.int32, shape, len(shape) - 1)
+
+
+def rows_of(shape):
+    return lax.broadcasted_iota(jnp.int32, shape, 0)
+
+
+def dot_f32(a, b, contract):
+    return lax.dot_general(a, b, (contract, ((), ())), preferred_element_type=jnp.float32)
+
+
+def retention_kernel(
+    chips,
+    query_wide,
+    key_wide,
+    value_wide,
+    query_narrow,
+    key_narrow,
+    value_narrow,
+    decay,
+    decay_t,
+    turns,
+    out_wide,
+    out_narrow,
+    residual,
+    gain,
+    hidden,
+    normed,
+    qbuf,
+    kbuf,
+    inner,
+    mixed,
+    pieces,
+    arrived,
+    answers,
+    states,
+    pbuf,
+    rbuf,
+    sbuf,
+    p1s,
+    p1r,
+    p2s,
+    p2r,
+    ds,
+    dr,
+    es,
+    er,
+):
+    z = lax.axis_index("sp_0")
+    c = lax.axis_index("sp_1")
+    x = lax.axis_index("tp")
+    nx = lax.axis_size("tp")
+    devices = chips * CORES
+    me = z * CORES + c
+    right = lax.rem(x + 1, nx)
+    left = lax.rem(x + nx - 1, nx)
+    length = query_wide.shape[0]
+    units = 4
+    lane = HEAD_WIDE
+    block = min(128, length)
+    f32 = jnp.float32
+    bf16 = jnp.bfloat16
+
+    def peer(step):
+        other = lax.rem(me + step, devices)
+        return other, {"sp_0": other // CORES, "sp_1": lax.rem(other, CORES)}
+
+    def at_x(xt):
+        return {"tp": xt}
+
+    barrier = pltpu.get_barrier_semaphore()
+    pl.semaphore_signal(barrier, inc=1, device_id=at_x(right), device_id_type=MESH)
+    pl.semaphore_signal(barrier, inc=1, device_id=at_x(left), device_id_type=MESH)
+
+    @pl.loop(1, devices)
+    def _(step):
+        pl.semaphore_signal(barrier, inc=1, device_id=peer(step)[1], device_id_type=MESH)
+
+    below = (
+        rows_of((length, length)) >= lanes_of((length, length))
+    ).astype(f32).astype(bf16)
+    cum = sum(dot_f32(below, term, ((1,), (0,))) for term in in_three(decay[...]))
+    cum_t = sum(dot_f32(term, below, ((1,), (1,))) for term in in_three(decay_t[...]))
+
+    table_lane = lanes_of((length, lane))
+    cos_all = turns[:, :lane]
+    sin_all = turns[:, lane:]
+    low = table_lane < HEAD_WIDE // 2
+
+    def wide_table(table):
+        return jnp.where(low, table, pltpu.roll(table, HEAD_WIDE // 2, 1))
+
+    def narrow_table(table):
+        first = pltpu.roll(table, 64, 1)
+        twice = jnp.where(table_lane < 32, first, pltpu.roll(first, 32, 1))
+        return jnp.where(low, twice, pltpu.roll(twice, 64, 1))
+
+    wide_cos = wide_table(cos_all)
+    wide_sin = wide_table(sin_all)
+    wide_sin = jnp.where(low, -wide_sin, wide_sin)
+    narrow_cos = narrow_table(cos_all)
+    narrow_sin = narrow_table(sin_all)
+    narrow_low = lax.rem(table_lane, HEAD_NARROW) < HEAD_NARROW // 2
+    narrow_sin = jnp.where(narrow_low, -narrow_sin, narrow_sin)
+
+    def turned(source, unit):
+        wide = unit < 2
+        lanes = slice((unit % 2) * lane, (unit % 2 + 1) * lane)
+        values = source[:, lanes].astype(f32)
+        if wide:
+            return values * wide_cos + pltpu.roll(values, HEAD_WIDE // 2, 1) * wide_sin
+        swapped = jnp.where(
+            narrow_low,
+            pltpu.roll(values, lane - HEAD_NARROW // 2, 1),
+            pltpu.roll(values, HEAD_NARROW // 2, 1),
+        )
+        return values * narrow_cos + swapped * narrow_sin
+
+    def values_of(unit):
+        source = value_wide if unit < 2 else value_narrow
+        return source[:, (unit % 2) * lane : (unit % 2 + 1) * lane]
+
+    def heads_of(unit):
+        return (unit,) if unit < 2 else (2 * unit - 2, 2 * unit - 1)
+
+    def per_lane(unit, column):
+        heads = heads_of(unit)
+        if len(heads) == 1:
+            return column(heads[0])
+        shape = (column(heads[0]).shape[0], lane)
+        return jnp.where(lanes_of(shape) < HEAD_NARROW, column(heads[0]), column(heads[1]))
+
+    def total_of(head):
+        return cum_t[head : head + 1, length - 1 : length]
+
+    unit_shape = (lane, lane)
+    unit_low_row = rows_of(unit_shape) < HEAD_NARROW
+    unit_low_lane = lanes_of(unit_shape) < HEAD_NARROW
+    local = []
+    for unit in range(units):
+        width = HEAD_WIDE if unit < 2 else HEAD_NARROW
+        key = (turned(key_wide if unit < 2 else key_narrow, unit) * width ** (-0.5)).astype(bf16)
+        kbuf[unit] = key
+        weight = per_lane(unit, lambda h: jnp.exp(total_of(h) - cum[:, h : h + 1]))
+        weighted = (key.astype(f32) * weight).astype(bf16)
+        state = dot_f32(weighted, values_of(unit), ((0,), (0,)))
+        if unit < 2:
+            local.append(state)
+        else:
+            packed = jnp.where(unit_low_row, state, pltpu.roll(state, HEAD_NARROW, 1))
+            wide_total = total_of(unit - 2)
+            narrow_total = jnp.where(
+                unit_low_row, total_of(heads_of(unit)[0]), total_of(heads_of(unit)[1])
+            )
+            lane_id = lanes_of(unit_shape)
+            for position, term in enumerate(
+                in_three(jnp.broadcast_to(wide_total, unit_shape)) + in_three(narrow_total)
+            ):
+                packed = jnp.where(
+                    lane_id == HEAD_NARROW + position, term.astype(f32), packed
+                )
+            local.append(packed)
+    piece_rows = 2 * lane // devices
+    for unit in range(units):
+        here = slice((unit % 2) * (devices // 2), (unit % 2 + 1) * (devices // 2))
+        lanes = slice((unit // 2) * lane, (unit // 2 + 1) * lane)
+        pieces[here, :, lanes] = local[unit].reshape(devices // 2, piece_rows, lane).astype(bf16)
+
+    pl.semaphore_wait(barrier, 2 + devices - 1)
+
+    def piece_out(step):
+        other, where = peer(step)
+        return pltpu.make_async_remote_copy(
+            src_ref=pieces.at[other],
+            dst_ref=arrived.at[me],
+            send_sem=p1s.at[step],
+            recv_sem=p1r.at[step],
+            device_id=where,
+            device_id_type=MESH,
+        )
+
+    def answer_out(step):
+        other, where = peer(step)
+        return pltpu.make_async_remote_copy(
+            src_ref=answers.at[other],
+            dst_ref=states.at[me],
+            send_sem=p2s.at[step],
+            recv_sem=p2r.at[step],
+            device_id=where,
+            device_id_type=MESH,
+        )
+
+    @pl.loop(1, devices)
+    def _(step):
+        piece_out(step).start()
+
+    arrived[me] = pieces[me]
+
+    for unit in range(units):
+        qbuf[unit] = turned(query_wide if unit < 2 else query_narrow, unit).astype(bf16)
+
+    def within(unit):
+        for start in range(0, length, block):
+            stop = start + block
+            shape = (block, stop)
+            causal = rows_of(shape) + start >= lanes_of(shape)
+            query = qbuf[unit, start:stop]
+            key = kbuf[unit, :stop]
+            value = values_of(unit)[:stop]
+            outs = []
+            for n, head in enumerate(heads_of(unit)):
+                own = query
+                if unit >= 2:
+                    mine = lax.div(lanes_of((block, lane)), HEAD_NARROW) == n
+                    own = jnp.where(mine, query.astype(f32), 0.0).astype(bf16)
+                scores = dot_f32(own, key, ((1,), (1,)))
+                gaps = cum[start:stop, head : head + 1] - cum_t[head : head + 1, :stop]
+                faded = scores * jnp.exp(jnp.where(causal, gaps, -jnp.inf))
+                outs.append(dot_f32(faded.astype(bf16), value, ((1,), (0,))))
+            if unit >= 2:
+                outs = [jnp.where(lanes_of((block, lane)) < HEAD_NARROW, outs[0], outs[1])]
+            inner[unit, start:stop] = outs[0]
+
+    for unit in range(2):
+        within(unit)
+
+    @pl.loop(1, devices)
+    def _(step):
+        piece_out(step).wait_recv()
+
+    running = jnp.zeros((piece_rows, 2 * lane), f32)
+    piece_lane = lanes_of((piece_rows, lane))
+    for source in range(devices):
+        answers[source] = running.astype(bf16)
+        came = arrived[source].astype(f32)
+        tail = came[:, lane:]
+
+        def log_at(first):
+            terms = (piece_lane >= first) & (piece_lane < first + 3)
+            return jnp.sum(jnp.where(terms, tail, 0.0), axis=1, keepdims=True)
+
+        scale = jnp.concatenate(
+            [
+                jnp.broadcast_to(jnp.exp(log_at(HEAD_NARROW)), piece_lane.shape),
+                jnp.broadcast_to(jnp.exp(log_at(HEAD_NARROW + 3)), piece_lane.shape),
+            ],
+            axis=1,
+        )
+        running = scale * running + came
+
+    @pl.loop(1, devices)
+    def _(step):
+        answer_out(step).start()
+
+    states[me] = answers[me]
+
+    for unit in range(2, units):
+        within(unit)
+
+    @pl.loop(1, devices)
+    def _(step):
+        answer_out(step).wait_recv()
+
+    for unit in range(units):
+        here = slice((unit % 2) * (devices // 2), (unit % 2 + 1) * (devices // 2))
+        lanes = slice((unit // 2) * lane, (unit // 2 + 1) * lane)
+        state = states[here, :, lanes].astype(f32).reshape(lane, lane)
+        if unit >= 2:
+            state = jnp.where(
+                unit_low_row,
+                jnp.where(unit_low_lane, state, 0.0),
+                jnp.where(unit_low_lane, 0.0, pltpu.roll(state, HEAD_NARROW, 1)),
+            )
+        carried = dot_f32(qbuf[unit], state.astype(bf16), ((1,), (0,)))
+        kept = per_lane(unit, lambda h: jnp.exp(cum[:, h : h + 1]))
+        value = inner[unit] + kept * carried
+
+        def mean_of(entries):
+            if unit < 2:
+                return jnp.mean(entries, axis=1, keepdims=True)
+            first = jnp.sum(jnp.where(low, entries, 0.0), axis=1, keepdims=True)
+            second = jnp.sum(jnp.where(low, 0.0, entries), axis=1, keepdims=True)
+            return jnp.where(low, first, second) * (1.0 / HEAD_NARROW)
+
+        centered = value - mean_of(value)
+        spread = mean_of(centered * centered)
+        mixed[:, unit * lane : (unit + 1) * lane] = (
+            centered * lax.rsqrt(spread + norm_eps)
+        ).astype(bf16)
+
+    rows_dev = length // nx
+    model_width = out_wide.shape[1]
+    half_model = model_width // 2
+
+    def x_copy(src, dst, send_sem, recv_sem, side):
+        return pltpu.make_async_remote_copy(
+            src_ref=src,
+            dst_ref=dst,
+            send_sem=send_sem,
+            recv_sem=recv_sem,
+            device_id=at_x(right if side == 0 else left),
+            device_id_type=MESH,
+        )
+
+    def far_half(side):
+        return x_copy(pbuf.at[3, side], rbuf.at[side], ds.at[side], dr.at[side], side)
+
+    def plain_half(side):
+        return x_copy(
+            pbuf.at[2 - side, 1 - side], sbuf.at[side, 1 - side], es.at[side, 0], er.at[side, 0], side
+        )
+
+    def added_half(side):
+        return x_copy(
+            pbuf.at[2 - side, side], sbuf.at[side, side], es.at[side, 1], er.at[side, 1], side
+        )
+
+    out_step = min(512, half_model)
+
+    def project(part, side):
+        target = (x, left, right, lax.rem(x + 2, nx))[part]
+        own_rows = pl.ds(pl.multiple_of(target * rows_dev, rows_dev), rows_dev)
+
+        @pl.loop(0, half_model // out_step)
+        def _(n):
+            cols = pl.ds(pl.multiple_of(side * half_model + n * out_step, out_step), out_step)
+            here = pl.ds(pl.multiple_of(n * out_step, out_step), out_step)
+            both = jnp.dot(
+                mixed[own_rows, : 2 * lane], out_wide[:, cols], preferred_element_type=f32
+            ) + jnp.dot(
+                mixed[own_rows, 2 * lane :], out_narrow[:, cols], preferred_element_type=f32
+            )
+            pbuf[part, side, :, here] = both.astype(bf16)
+
+    for side in range(2):
+        project(3, side)
+        far_half(side).start()
+    for side in range(2):
+        project(2 - side, 1 - side)
+        plain_half(side).start()
+    for side in range(2):
+        project(2 - side, side)
+    for side in range(2):
+        project(0, side)
+    for side in range(2):
+        far_half(side).wait_recv()
+        pbuf[2 - side, side] = (
+            pbuf[2 - side, side].astype(f32) + rbuf[side].astype(f32)
+        ).astype(bf16)
+        added_half(side).start()
+    for side in range(2):
+        plain_half(side).wait_recv()
+        added_half(side).wait_recv()
+    squares = jnp.zeros((rows_dev, 1), f32)
+    for h in range(2):
+        cols = slice(h * half_model, (h + 1) * half_model)
+        stream = residual[:, cols].astype(f32) + (
+            pbuf[0, h].astype(f32) + sbuf[0, h].astype(f32) + sbuf[1, h].astype(f32)
+        )
+        hidden[:, cols] = stream
+        squares = squares + jnp.sum(stream * stream, axis=1, keepdims=True)
+    scale_row = lax.rsqrt(squares * (1.0 / model_width) + norm_eps)
+    normed[...] = (hidden[...] * scale_row * gain[...]).astype(bf16)
+
+    @pl.loop(1, devices)
+    def _(step):
+        piece_out(step).wait_send()
+        answer_out(step).wait_send()
+
+    for side in range(2):
+        far_half(side).wait_send()
+        plain_half(side).wait_send()
+        added_half(side).wait_send()
+
+
+def retention_stage(
+    query_wide,
+    key_wide,
+    value_wide,
+    decay_wide,
+    query_narrow,
+    key_narrow,
+    value_narrow,
+    decay_narrow,
+    residual,
+    out_wide,
+    out_narrow,
+    norm_gain,
+):
+    length = query_wide.shape[0]
+    chips = lax.axis_size("sp_0")
+    devices = chips * CORES
+    rows_dev, model_width = residual.shape
+    decay = jnp.concatenate(
+        [decay_wide, decay_narrow, jnp.zeros((length, 2), jnp.float32)], axis=1
+    )
+    positions = (lax.axis_index(SP) * length + jnp.arange(length, dtype=jnp.int32)).astype(
+        jnp.float32
+    )
+    inverse = [
+        rotary_base ** (-jnp.arange(width // 2, dtype=jnp.float32) / (width // 2))
+        for width in (HEAD_WIDE, HEAD_NARROW)
+    ]
+    inverse = jnp.concatenate(inverse + [jnp.zeros((HEAD_NARROW // 2,), jnp.float32)])
+    angles = positions[:, None] * inverse[None, :]
+    turns = jnp.concatenate([jnp.cos(angles), jnp.sin(angles)], axis=1)
+    vmem = pl.BlockSpec(memory_space=pltpu.VMEM)
+    bf16 = jnp.bfloat16
+    dma = pltpu.SemaphoreType.DMA
+    piece_rows = 2 * HEAD_WIDE // devices
+    moved = pltpu.VMEM((devices, piece_rows, 2 * HEAD_WIDE), bf16)
+    return pl.pallas_call(
+        functools.partial(retention_kernel, chips),
+        out_shape=(
+            jax.ShapeDtypeStruct(residual.shape, jnp.float32),
+            jax.ShapeDtypeStruct(residual.shape, bf16),
+        ),
+        in_specs=[vmem] * 13,
+        out_specs=(vmem, vmem),
+        scratch_shapes=[
+            pltpu.VMEM((4, length, HEAD_WIDE), bf16),
+            pltpu.VMEM((4, length, HEAD_WIDE), bf16),
+            pltpu.VMEM((4, length, HEAD_WIDE), jnp.float32),
+            pltpu.VMEM((length, 4 * HEAD_WIDE), bf16),
+            moved,
+            moved,
+            moved,
+            moved,
+            pltpu.VMEM((4, 2, rows_dev, model_width // 2), bf16),
+            pltpu.VMEM((2, rows_dev, model_width // 2), bf16),
+            pltpu.VMEM((2, 2, rows_dev, model_width // 2), bf16),
+            dma((devices,)),
+            dma((devices,)),
+            dma((devices,)),
+            dma((devices,)),
+            dma((2,)),
+            dma((2,)),
+            dma((2, 2)),
+            dma((2, 2)),
+        ],
+        compiler_params=pltpu.CompilerParams(
+            collective_id=1, has_side_effects=True, vmem_limit_bytes=40 * 1024 * 1024
+        ),
+        name="retention_stage",
+    )(
+        query_wide,
+        key_wide,
+        value_wide,
+        query_narrow,
+        key_narrow,
+        value_narrow,
+        decay,
+        decay.T,
+        turns,
+        out_wide,
+        out_narrow,
+        residual,
+        norm_gain[None, :],
+    )
+
+
 def body(
     query_wide,
     key_wide,
@@ -605,34 +952,22 @@
     expert_up,
     expert_down,
 ):
-    length = query_wide.shape[0]
-    tp_count = lax.axis_size("tp")
     experts = lax.axis_size(SP)
-    model_width = residual.shape[1]
-    positions = (lax.axis_index(SP) * length + jnp.arange(length, dtype=jnp.int32)).astype(
-        jnp.float32
+    rows_dev, model_width = residual.shape
+    hidden_state, normed = retention_stage(
+        query_wide,
+        key_wide,
+        value_wide,
+        decay_wide,
+        query_narrow,
+        key_narrow,
+        value_narrow,
+        decay_narrow,
+        residual,
+        out_wide,
+        out_narrow,
+        norm_gain,
     )
-    wide_parts = local_terms(query_wide, key_wide, value_wide, decay_wide, HEAD_WIDE, positions)
-    narrow_parts = local_terms(
-        query_narrow, key_narrow, value_narrow, decay_narrow, HEAD_NARROW, positions
-    )
-    local_states = (wide_parts[3], wide_parts[4], narrow_parts[3], narrow_parts[4])
-    identity = tuple((jnp.zeros_like(member) for member in local_states))
-    carried = prefix_by_axis(local_states, SP, combine, identity)
-    mixed_wide = finish(wide_parts, carried[1])
-    mixed_narrow = finish(narrow_parts, carried[3])
-    rows_dev = length // tp_count
-    attention = sent_and_summed(
-        (
-            jnp.dot(mixed_wide, out_wide, preferred_element_type=jnp.float32)
-            + jnp.dot(mixed_narrow, out_narrow, preferred_element_type=jnp.float32)
-        ).astype(jnp.bfloat16),
-        "tp",
-        0,
-    )
-    hidden_state = residual.astype(jnp.float32) + attention
-    scale_row = lax.rsqrt(jnp.mean(hidden_state * hidden_state, axis=-1, keepdims=True) + norm_eps)
-    normed = (hidden_state * scale_row * norm_gain).astype(jnp.bfloat16)
     capacity = max(2, 3 * rows_dev * TOP_K // (2 * experts))
     flat_expert = routes.reshape(-1)
     one_hot = (flat_expert[:, None] == jnp.arange(experts, dtype=jnp.int32)[None, :]).astype(

time: 357 us -> 249 us (0.70)
  blocking collectives: 99.7 us -> 0 us
  Pallas kernels: 177 us -> 231 us
  matrix products: 18.9 us -> 3.06 us
  between operations: 14 us -> 0.23 us
  waiting for transfers between devices: 13 us -> 0 us
  other arithmetic: 14 us -> 3.66 us
  starting transfers between devices: 5.2 us -> 0 us
  local copies, waits for them, and re-layouts: 13.6 us -> 9.37 us
    all_gather x7 -> x0, blocking collectives: 99.7 us -> none  [prefix_by_axis(): lax.all_gather(part.astype(kind), axis)]
    pallas_call x0 -> x1, Pallas kernels: none -> 70.5 us  [retention_stage(): pl.pallas_call(functools.partial(retention_kernel, chips), out_shape=(jax...]
    pallas_call x1, Pallas kernels: 177 us -> 160 us  [experts_stage(): pl.pallas_call(functools.partial(experts_kernel, chips), out_shape=jax.Sh...]
    dot_general x8 -> x0, matrix products: 15.5 us -> none  [the longest x2 6.17 us: local_terms(): inner_part = jnp.einsum('hts,she->the', scores, value_f)]
    all_to_all x1 -> x0, waiting for transfers between devices: 13 us -> none  [sent_and_summed(): lax.all_to_all(pieces, axis, split_axis=0, concat_axis=0, tiled=True)]
    all_to_all x1 -> x0, starting transfers between devices: 5.2 us -> none  [sent_and_summed(): lax.all_to_all(pieces, axis, split_axis=0, concat_axis=0, tiled=True)]
    unnamed x78 -> x30, local copies, waits for them, and re-layouts: 6.17 us -> 8.3 us
  transfers between devices with their start and end apart: 2 -> 0, of which waited for: 1 -> 0; matrix products, arithmetic and copies ran while one was open for 6% -> 0% of each run, Pallas kernels for 0% -> 0%
where the time goes in v2:
time: 249 us; the launch traced here: 247 us
  Pallas kernels  231 us (93%)
  local copies, waits for them, and re-layouts  9.37 us (4%)
  other arithmetic  3.66 us (1%)
  matrix products  3.06 us (1%)
    pallas_call x1, Pallas kernels, experts_stage(): pl.pallas_call(functools.partial(experts_kernel, chips), out_shape=jax.Sh...  160 us
    pallas_call x1, Pallas kernels, retention_stage(): pl.pallas_call(functools.partial(retention_kernel, chips), out_shape=(jax...  70.5 us
    unnamed x30, local copies, waits for them, and re-layouts  8.3 us

profile of v2, /device:TPU:33, one launch (start us, length us, event | category | flops | bytes accessed | tf_op | source)
XLA Modules:
  0.0 247.3 jit_solution(10338883574930668852)
XLA Ops:
  0.1 0.9 fusion.28
  1.0 0.1 copy.33.decay
  1.2 1.0 multiply_cosine_fusion
  2.3 1.2 copy-done.2
  3.5 0.9 copy-done.5
  4.5 0.9 copy-done.6
  5.4 0.9 copy-done.7
  6.4 0.9 copy-done.8
  7.3 0.9 copy-done.9
  8.3 0.9 copy-done.10
  9.2 0.7 copy-done.11
  9.9 70.5 %retention_stage.1 = (f32[128,2048]{1,0:T(8,128)S(1)}, bf16[128,2048]{1,0:T(8,128)(2,1)S(1)}) custom-call(bf16[512,256]{1,0:T(8,128)(2,1)S(1)} %copy-done.5, bf16[512,256]{1,0:T(8,128)(2,1)S(1)} %copy-done.6, bf16[512,256]{1,0:T(8,128)(2,1)S(1)} %copy-done.7, bf16[512,256]{1,0:T(8,128)(2,1)S(1)} %copy-done.8, bf16[512,256]{1,0:T(8,128)(2,1)S(1)} %copy-done.9, ...), custom_call_target="tpu_custom_call" | custom-call | tf_op jit(solution)/shard_map/retention_stage/pallas_call | solution.py:886
  80.5 0.1 copy.34
  80.6 0.1 eq.81
  80.7 0.1 eq.85
  80.9 0.6 reduce-window.6
  81.5 0.2 slice_reduce_fusion
  81.8 0.1 reduce_sum.12
  82.2 1.0 fusion.5
  83.2 0.5 copy-done
  83.8 160.4 %experts_stage.1 = bf16[32,48,512]{2,1,0:T(8,128)(2,1)S(1)} custom-call(bf16[32,48,512]{2,1,0:T(8,128)(2,1)S(1)} %bitcast.50, bf16[192,192]{1,0:T(8,128)(2,1)S(1)} %copy-done.4, bf16[192,192]{1,0:T(8,128)(2,1)S(1)} %copy-done.4, bf16[2048,512]{1,0:T(8,128)(2,1)S(1)} %bitcast.47, bf16[2048,512]{1,0:T(8,128)(2,1)} %bitcast.52, bf16[512,2048]{1,0:T(8,128)(2,1)} %bitcast.53), custom_call_target="tpu_custom_call" | custom-call | tf_op jit(solution)/shard_map/experts_stage/pallas_call | solution.py:429
  244.3 1.0 fusion.12
  245.3 1.0 fusion.14
  246.4 0.9 fusion.15
  (42 shorter events, 0.7 us)
Async XLA Ops:
  0.0 2.3 copy-start.1
  0.0 2.3 copy-start.3
  2.3 1.2 copy-start.2
  3.5 0.9 copy-start.5
  4.5 0.9 copy-start.6
  5.4 0.9 copy-start.7
  6.4 0.9 copy-start.8
  7.3 0.9 copy-start.9
  8.3 0.9 copy-start.10
  9.2 0.7 copy-start.11
  9.9 70.6 %copy-start.12 = (s32[128,2]{0,1:T(2,128)S(1)}, s32[128,2]{0,1:T(2,128)}, u32[]{:S(2)}) copy-start(s32[128,2]{0,1:T(2,128)} %param.31) | copy-start | bytes 3076
  82.2 1.6 copy-start
  82.2 1.6 copy-start.4
  83.8 160.5 %copy-start.13 = (f32[128,2]{0,1:T(2,128)S(1)}, f32[128,2]{0,1:T(2,128)}, u32[]{:S(2)}) copy-start(f32[128,2]{0,1:T(2,128)} %param.32) | copy-start | bytes 3076

commit v3 on v1

v3 whole, which is shorter than its diff:
```python
import functools

import jax
import jax.numpy as jnp
import numpy as np
from jax import lax
from jax.experimental import pallas as pl
from jax.experimental.pallas import tpu as pltpu
from jax.sharding import Mesh
from jax.sharding import PartitionSpec as P

HEAD_WIDE = 128
HEAD_NARROW = 64
TOP_K = 2
SP = ("sp_0", "sp_1")
GRP_SP = ("grp", "sp_0", "sp_1")
GRP_SP_TP = ("grp", "sp_0", "sp_1", "tp")


norm_eps = 1e-05
clamp_limit = 7.0
swish_alpha = 1.702
rotary_base = 10000.0


def activate(gate_pre, up_pre):
    gate_clip = jnp.minimum(gate_pre, clamp_limit)
    up_clip = jnp.clip(up_pre, -clamp_limit, clamp_limit)
    return gate_clip * jax.nn.sigmoid(swish_alpha * gate_clip) * (up_clip + 1.0)


QUARTERS = 4
CORES = 2
MESH = pl.DeviceIdType.MESH


def regroup(capacity):
    rows = 4 * QUARTERS * capacity
    table = np.zeros((rows, rows), np.float32)
    for block in range(4):
        for part in range(QUARTERS):
            for row in range(capacity):
                table[
                    (part * 4 + block) * capacity + row, (block * QUARTERS + part) * capacity + row
                ] = 1.0
    return table


def in_three(value):
    first = value.astype(jnp.bfloat16)
    rest = value - first.astype(jnp.float32)
    second = rest.astype(jnp.bfloat16)
    third = (rest - second.astype(jnp.float32)).astype(jnp.bfloat16)
    return (first, second, third)


def lanes_of(shape):
    return lax.broadcasted_iota(jnp.int32, shape, len(shape) - 1)


def rows_of(shape):
    return lax.broadcasted_iota(jnp.int32, shape, 0)


def dot_f32(a, b, contract):
    return lax.dot_general(a, b, (contract, ((), ())), preferred_element_type=jnp.float32)


def layer_kernel(
    chips,
    decay,
    decay_t,
    turns,
    gain,
    routes,
    route_weights,
    perm,
    perm_back,
    query_wide_hbm,
    key_wide_hbm,
    value_wide_hbm,
    query_narrow_hbm,
    key_narrow_hbm,
    value_narrow_hbm,
    out_wide_hbm,
    out_narrow_hbm,
    residual_hbm,
    gate_hbm,
    up_hbm,
    down_hbm,
    out,
    query_wide,
    key_wide,
    value_wide,
    query_narrow,
    key_narrow,
    value_narrow,
    out_wide,
    out_narrow,
    residual,
    gate,
    up,
    down,
    hidden,
    parted,
    chosen,
    picks,
    send,
    back,
    qbuf,
    kbuf,
    inner,
    mixed,
    pieces,
    arrived,
    answers,
    states,
    proj,
    proj_far,
    proj_sum,
    gbuf,
    xbuf,
    hbuf,
    pbuf,
    rbuf,
    sbuf,
    ret,
    load_sem,
    p1s,
    p1r,
    p2s,
    p2r,
    pds,
    pdr,
    pes,
    per,
    zs,
    zr,
    xs,
    xr,
    ys,
    yr,
    ds,
    dr,
    es,
    er,
    rs,
    rr,
):
    z = lax.axis_index("sp_0")
    c = lax.axis_index("sp_1")
    x = lax.axis_index("tp")
    nx = lax.axis_size("tp")
    devices = chips * CORES
    me = z * CORES + c
    right = lax.rem(x + 1, nx)
    left = lax.rem(x + nx - 1, nx)
    length = query_wide.shape[0]
    units = 4
    lane = HEAD_WIDE
    block = min(128, length)
    f32 = jnp.float32
    bf16 = jnp.bfloat16

    def peer(step):
        other = lax.rem(me + step, devices)
        return other, {"sp_0": other // CORES, "sp_1": lax.rem(other, CORES)}

    def at_x(xt):
        return {"tp": xt}

    loads = [
        pltpu.make_async_copy(source, target, load_sem.at[n])
        for n, (source, target) in enumerate(
            (
                (key_wide_hbm, key_wide),
                (key_narrow_hbm, key_narrow),
                (value_wide_hbm, value_wide),
                (value_narrow_hbm, value_narrow),
                (query_wide_hbm, query_wide),
                (query_narrow_hbm, query_narrow),
                (out_wide_hbm, out_wide),
                (out_narrow_hbm, out_narrow),
                (residual_hbm, residual),
                (gate_hbm, gate),
                (up_hbm, up),
                (down_hbm, down),
            )
        )
    ]
    for load in loads[:6]:
        load.start()

    barrier = pltpu.get_barrier_semaphore()
    pl.semaphore_signal(barrier, inc=1, device_id=at_x(right), device_id_type=MESH)
    pl.semaphore_signal(barrier, inc=1, device_id=at_x(left), device_id_type=MESH)

    @pl.loop(1, devices)
    def _(step):
        pl.semaphore_signal(barrier, inc=1, device_id=peer(step)[1], device_id_type=MESH)

    for load in loads[6:]:
        load.start()

    square = (length, length)
    below = (rows_of(square) >= lanes_of(square)).astype(f32).astype(bf16)
    cum = sum(dot_f32(below, term, ((1,), (0,))) for term in in_three(decay[...]))
    cum_t = sum(dot_f32(term, below, ((1,), (1,))) for term in in_three(decay_t[...]))

    table_lane = lanes_of((length, lane))
    cos_all = turns[:, :lane]
    sin_all = turns[:, lane:]
    low = table_lane < HEAD_WIDE // 2

    def wide_table(table):
        return jnp.where(low, table, pltpu.roll(table, HEAD_WIDE // 2, 1))

    def narrow_table(table):
        first = pltpu.roll(table, 64, 1)
        twice = jnp.where(table_lane < 32, first, pltpu.roll(first, 32, 1))
        return jnp.where(low, twice, pltpu.roll(twice, 64, 1))

    wide_cos = wide_table(cos_all)
    wide_sin = wide_table(sin_all)
    wide_sin = jnp.where(low, -wide_sin, wide_sin)
    narrow_cos = narrow_table(cos_all)
    narrow_sin = narrow_table(sin_all)
    narrow_low = lax.rem(table_lane, HEAD_NARROW) < HEAD_NARROW // 2
    narrow_sin = jnp.where(narrow_low, -narrow_sin, narrow_sin)

    def turned(source, unit):
        wide = unit < 2
        lanes = slice((unit % 2) * lane, (unit % 2 + 1) * lane)
        values = source[:, lanes].astype(f32)
        if wide:
            return values * wide_cos + pltpu.roll(values, HEAD_WIDE // 2, 1) * wide_sin
        swapped = jnp.where(
            narrow_low,
            pltpu.roll(values, lane - HEAD_NARROW // 2, 1),
            pltpu.roll(values, HEAD_NARROW // 2, 1),
        )
        return values * narrow_cos + swapped * narrow_sin

    def values_of(unit):
        source = value_wide if unit < 2 else value_narrow
        return source[:, (unit % 2) * lane : (unit % 2 + 1) * lane]

    def heads_of(unit):
        return (unit,) if unit < 2 else (2 * unit - 2, 2 * unit - 1)

    def per_lane(unit, column):
        heads = heads_of(unit)
        if len(heads) == 1:
            return column(heads[0])
        shape = (column(heads[0]).shape[0], lane)
        return jnp.where(lanes_of(shape) < HEAD_NARROW, column(heads[0]), column(heads[1]))

    def total_of(head):
        return cum_t[head : head + 1, length - 1 : length]

    unit_shape = (lane, lane)
    unit_low_row = rows_of(unit_shape) < HEAD_NARROW
    unit_low_lane = lanes_of(unit_shape) < HEAD_NARROW
    for load in loads[:4]:
        load.wait()
    local = []
    for unit in range(units):
        width = HEAD_WIDE if unit < 2 else HEAD_NARROW
        key = (turned(key_wide if unit < 2 else key_narrow, unit) * width ** (-0.5)).astype(bf16)
        kbuf[unit] = key
        weight = per_lane(unit, lambda h: jnp.exp(total_of(h) - cum[:, h : h + 1]))
        weighted = (key.astype(f32) * weight).astype(bf16)
        state = dot_f32(weighted, values_of(unit), ((0,), (0,)))
        if unit < 2:
            local.append(state)
        else:
            packed = jnp.where(unit_low_row, state, pltpu.roll(state, HEAD_NARROW, 1))
            wide_total = total_of(unit - 2)
            narrow_total = jnp.where(
                unit_low_row, total_of(heads_of(unit)[0]), total_of(heads_of(unit)[1])
            )
            lane_id = lanes_of(unit_shape)
            for position, term in enumerate(
                in_three(jnp.broadcast_to(wide_total, unit_shape)) + in_three(narrow_total)
            ):
                packed = jnp.where(
                    lane_id == HEAD_NARROW + position, term.astype(f32), packed
                )
            local.append(packed)
    piece_rows = 2 * lane // devices
    for unit in range(units):
        here = slice((unit % 2) * (devices // 2), (unit % 2 + 1) * (devices // 2))
        lanes = slice((unit // 2) * lane, (unit // 2 + 1) * lane)
        pieces[here, :, lanes] = local[unit].reshape(devices // 2, piece_rows, lane).astype(bf16)

    pl.semaphore_wait(barrier, 2 + devices - 1)

    def piece_out(step):
        other, where = peer(step)
        return pltpu.make_async_remote_copy(
            src_ref=pieces.at[other],
            dst_ref=arrived.at[me],
            send_sem=p1s.at[step],
            recv_sem=p1r.at[step],
            device_id=where,
            device_id_type=MESH,
        )

    def answer_out(step):
        other, where = peer(step)
        return pltpu.make_async_remote_copy(
            src_ref=answers.at[other],
            dst_ref=states.at[me],
            send_sem=p2s.at[step],
            recv_sem=p2r.at[step],
            device_id=where,
            device_id_type=MESH,
        )

    @pl.loop(1, devices)
    def _(step):
        piece_out(step).start()

    arrived[me] = pieces[me]

    for load in loads[4:6]:
        load.wait()
    for unit in range(units):
        qbuf[unit] = turned(query_wide if unit < 2 else query_narrow, unit).astype(bf16)

    def within(unit):
        for start in range(0, length, block):
            stop = start + block
            shape = (block, stop)
            causal = rows_of(shape) + start >= lanes_of(shape)
            query = qbuf[unit, start:stop]
            key = kbuf[unit, :stop]
            value = values_of(unit)[:stop]
            outs = []
            for n, head in enumerate(heads_of(unit)):
                own = query
                if unit >= 2:
                    mine = lax.div(lanes_of((block, lane)), HEAD_NARROW) == n
                    own = jnp.where(mine, query.astype(f32), 0.0).astype(bf16)
                scores = dot_f32(own, key, ((1,), (1,)))
                gaps = cum[start:stop, head : head + 1] - cum_t[head : head + 1, :stop]
                faded = scores * jnp.exp(jnp.where(causal, gaps, -jnp.inf))
                outs.append(dot_f32(faded.astype(bf16), value, ((1,), (0,))))
            if unit >= 2:
                outs = [jnp.where(lanes_of((block, lane)) < HEAD_NARROW, outs[0], outs[1])]
            inner[unit, start:stop] = outs[0]

    for unit in range(2):
        within(unit)

    @pl.loop(1, devices)
    def _(step):
        piece_out(step).wait_recv()

    running = jnp.zeros((piece_rows, 2 * lane), f32)
    piece_lane = lanes_of((piece_rows, lane))
    for source in range(devices):
        answers[source] = running.astype(bf16)
        came = arrived[source].astype(f32)
        tail = came[:, lane:]

        def log_at(first):
            terms = (piece_lane >= first) & (piece_lane < first + 3)
            return jnp.sum(jnp.where(terms, tail, 0.0), axis=1, keepdims=True)

        scale = jnp.concatenate(
            [
                jnp.broadcast_to(jnp.exp(log_at(HEAD_NARROW)), piece_lane.shape),
                jnp.broadcast_to(jnp.exp(log_at(HEAD_NARROW + 3)), piece_lane.shape),
            ],
            axis=1,
        )
        running = scale * running + came

    @pl.loop(1, devices)
    def _(step):
        answer_out(step).start()

    states[me] = answers[me]

    for unit in range(2, units):
        within(unit)

    @pl.loop(1, devices)
    def _(step):
        answer_out(step).wait_recv()

    for unit in range(units):
        here = slice((unit % 2) * (devices // 2), (unit % 2 + 1) * (devices // 2))
        lanes = slice((unit // 2) * lane, (unit // 2 + 1) * lane)
        state = states[here, :, lanes].astype(f32).reshape(lane, lane)
        if unit >= 2:
            state = jnp.where(
                unit_low_row,
                jnp.where(unit_low_lane, state, 0.0),
                jnp.where(unit_low_lane, 0.0, pltpu.roll(state, HEAD_NARROW, 1)),
            )
        carried = dot_f32(qbuf[unit], state.astype(bf16), ((1,), (0,)))
        kept = per_lane(unit, lambda h: jnp.exp(cum[:, h : h + 1]))
        value = inner[unit] + kept * carried

        def mean_of(entries):
            if unit < 2:
                return jnp.mean(entries, axis=1, keepdims=True)
            first = jnp.sum(jnp.where(low, entries, 0.0), axis=1, keepdims=True)
            second = jnp.sum(jnp.where(low, 0.0, entries), axis=1, keepdims=True)
            return jnp.where(low, first, second) * (1.0 / HEAD_NARROW)

        centered = value - mean_of(value)
        spread = mean_of(centered * centered)
        mixed[:, unit * lane : (unit + 1) * lane] = (
            centered * lax.rsqrt(spread + norm_eps)
        ).astype(bf16)

    rows_dev = length // nx
    model_width = out_wide.shape[1]
    proj_half = model_width // 2

    for load in loads[6:9]:
        load.wait()

    def x_copy(src, dst, send_sem, recv_sem, side):
        return pltpu.make_async_remote_copy(
            src_ref=src,
            dst_ref=dst,
            send_sem=send_sem,
            recv_sem=recv_sem,
            device_id=at_x(right if side == 0 else left),
            device_id_type=MESH,
        )

    def proj_far_half(side):
        return x_copy(proj.at[3, side], proj_far.at[side], pds.at[side], pdr.at[side], side)

    def proj_plain_half(side):
        return x_copy(
            proj.at[2 - side, 1 - side], proj_sum.at[side, 1 - side], pes.at[side, 0], per.at[side, 0], side
        )

    def proj_added_half(side):
        return x_copy(
            proj.at[2 - side, side], proj_sum.at[side, side], pes.at[side, 1], per.at[side, 1], side
        )

    out_step = min(512, proj_half)

    def project(part, side):
        target = (x, left, right, lax.rem(x + 2, nx))[part]
        own_rows = pl.ds(pl.multiple_of(target * rows_dev, rows_dev), rows_dev)

        @pl.loop(0, proj_half // out_step)
        def _(n):
            cols = pl.ds(pl.multiple_of(side * proj_half + n * out_step, out_step), out_step)
            here = pl.ds(pl.multiple_of(n * out_step, out_step), out_step)
            both = jnp.dot(
                mixed[own_rows, : 2 * lane], out_wide[:, cols], preferred_element_type=f32
            ) + jnp.dot(
                mixed[own_rows, 2 * lane :], out_narrow[:, cols], preferred_element_type=f32
            )
            proj[part, side, :, here] = both.astype(bf16)

    for side in range(2):
        project(3, side)
        proj_far_half(side).start()
    for side in range(2):
        project(2 - side, 1 - side)
        proj_plain_half(side).start()
    for side in range(2):
        project(2 - side, side)
    for side in range(2):
        project(0, side)
    for side in range(2):
        proj_far_half(side).wait_recv()
        proj[2 - side, side] = (
            proj[2 - side, side].astype(f32) + proj_far[side].astype(f32)
        ).astype(bf16)
        proj_added_half(side).start()
    experts = devices
    one_hots = []
    for k in range(TOP_K):
        wanted = jnp.broadcast_to(routes[:, k : k + 1], (rows_dev, experts))
        one_hots.append((wanted == lanes_of((rows_dev, experts))).astype(f32))
    rows_square = (rows_dev, rows_dev)
    above = (rows_of(rows_square) > lanes_of(rows_square)).astype(f32).astype(bf16)
    diagonal = rows_of(rows_square) == lanes_of(rows_square)
    before = jnp.zeros((1, experts), f32)
    parts = QUARTERS * rows_dev
    slots = send.shape[0] * send.shape[1]
    capacity = send.shape[1] // QUARTERS
    width = send.shape[2]
    picked_rows = []
    for k in range(TOP_K):
        ahead = dot_f32(above, one_hots[k].astype(bf16), ((1,), (0,))) + before
        rank = jnp.sum(ahead * one_hots[k], axis=1, keepdims=True)
        before = before + jnp.sum(one_hots[k], axis=0, keepdims=True)
        place = routes[:, k : k + 1].astype(f32) * float(QUARTERS * capacity) + rank
        across = jnp.sum(
            jnp.where(diagonal, jnp.broadcast_to(place, rows_square), 0.0), axis=0, keepdims=True
        )
        picked_rows.append(
            jnp.concatenate([across + float(q * capacity) for q in range(QUARTERS)], axis=1)
        )
        for q in range(QUARTERS):
            own = slice(q * rows_dev, (q + 1) * rows_dev)
            wanted = jnp.broadcast_to(place + float(q * capacity), (rows_dev, slots))
            picks[k, own] = (
                (wanted == lanes_of((rows_dev, slots)).astype(f32)).astype(f32).astype(bf16)
            )
    step_rows = slots // 4

    @pl.loop(0, 4)
    def _(n):
        first = pl.multiple_of(n * step_rows, step_rows)
        slot = (rows_of((step_rows, parts)) + first).astype(f32)
        hit = (slot == picked_rows[0]) | (slot == picked_rows[1])
        chosen[pl.ds(first, step_rows)] = hit.astype(f32).astype(bf16)

    for side in range(2):
        proj_plain_half(side).wait_recv()
        proj_added_half(side).wait_recv()
    squares = jnp.zeros((rows_dev, 1), f32)
    for h in range(2):
        cols = slice(h * proj_half, (h + 1) * proj_half)
        stream = residual[:, cols].astype(f32) + (
            proj[0, h].astype(f32) + proj_sum[0, h].astype(f32) + proj_sum[1, h].astype(f32)
        )
        hidden[:, cols] = stream
        squares = squares + jnp.sum(stream * stream, axis=1, keepdims=True)
    scale_row = lax.rsqrt(squares * (1.0 / model_width) + norm_eps)
    for q in range(QUARTERS):
        cols = slice(q * width, (q + 1) * width)
        parted[q * rows_dev : (q + 1) * rows_dev] = (
            hidden[:, cols] * scale_row * gain[:, cols]
        ).astype(bf16)
    step_experts = experts // 4

    @pl.loop(0, 4)
    def _(n):
        first = pl.multiple_of(n * step_rows, step_rows)
        taken = jnp.dot(
            chosen[pl.ds(first, step_rows)], parted[...], preferred_element_type=f32
        ).astype(bf16)
        send[pl.ds(n * step_experts, step_experts)] = taken.reshape(
            step_experts, QUARTERS * capacity, width
        )

    half = chips // 2
    groups = half
    last = groups - 1
    block_rows = send.shape[1]
    rows = 4 * capacity
    half_model = QUARTERS * width // 2
    hidden_width = gate.shape[1]

    def remote(src, dst, send_sem, recv_sem, to):
        return pltpu.make_async_remote_copy(
            src_ref=src,
            dst_ref=dst,
            send_sem=send_sem,
            recv_sem=recv_sem,
            device_id=to,
            device_id_type=MESH,
        )

    def at_z(zt, ct):
        return {"sp_0": zt, "sp_1": ct}

    def chip_at(offset):
        return lax.rem(z + offset + chips, chips)

    def partner_out():
        return remote(
            send.at[z * CORES + 1 - c], gbuf.at[0, last, c], zs.at[4 * last], zr.at[4 * last],
            at_z(z, 1 - c),
        )

    def far_out(ct):
        zt = chip_at(half)
        return remote(
            send.at[zt * CORES + ct],
            gbuf.at[0, last, 2 + c],
            zs.at[4 * last + 2 + ct],
            zr.at[4 * last + 2 + c],
            at_z(zt, ct),
        )

    def near_out(d, sign, ct):
        zt = chip_at(d) if sign == 0 else chip_at(-d)
        return remote(
            send.at[zt * CORES + ct],
            gbuf.at[0, d - 1, 2 * sign + c],
            zs.at[4 * (d - 1) + 2 * sign + ct],
            zr.at[4 * (d - 1) + 2 * sign + c],
            at_z(zt, ct),
        )

    partner_out().start()

    @pl.loop(1, half)
    def _(d):
        for ct in range(CORES):
            for sign in range(2):
                near_out(d, sign, ct).start()

    for ct in range(CORES):
        far_out(ct).start()
    gbuf[0, last, c] = send[me]
    for load in loads[9:]:
        load.wait()

    def z_arrived(g, j):
        return remote(send.at[0], gbuf.at[0, g, j], zs.at[0], zr.at[4 * g + j], at_z(z, 1 - c))

    def spread(side, g):
        return remote(
            gbuf.at[0, g],
            gbuf.at[1 + side, g],
            xs.at[side, g],
            xr.at[side, g],
            at_x(right if side == 0 else left),
        )

    def relay(side, g):
        return remote(
            gbuf.at[1 + side, g, pl.ds(2 * side, 2)],
            gbuf.at[3, g, pl.ds(2 * side, 2)],
            ys.at[side, g],
            yr.at[side, g],
            at_x(right if side == 0 else left),
        )

    def stage_a(g):
        @pl.when(g < last)
        def _():
            for j in range(4):
                z_arrived(g, j).wait_recv()

        @pl.when(g == last)
        def _():
            for j in (0, 2, 3):
                z_arrived(g, j).wait_recv()

        for side in range(2):
            spread(side, g).start()

    def stage_b(g):
        for side in range(2):
            spread(side, g).wait_recv()
            relay(side, g).start()

    def far_half(side, g):
        return remote(
            pbuf.at[g, 3, side],
            rbuf.at[side, g],
            ds.at[side, g],
            dr.at[side, g],
            at_x(right if side == 0 else left),
        )

    def plain_half(side, g):
        return remote(
            pbuf.at[g, 2 - side, 1 - side],
            sbuf.at[side, 1 - side, g],
            es.at[side, 0, g],
            er.at[side, 0, g],
            at_x(right if side == 0 else left),
        )

    def added_half(side, g):
        return remote(
            pbuf.at[g, 2 - side, side],
            sbuf.at[side, side, g],
            es.at[side, 1, g],
            er.at[side, 1, g],
            at_x(right if side == 0 else left),
        )

    def stage_c(g):
        for side in range(2):
            relay(side, g).wait_recv()
        for part in range(4):
            block = gbuf[part, g].reshape(4 * block_rows, width)
            turned = jnp.dot(perm[...], block, preferred_element_type=jnp.float32).astype(
                jnp.bfloat16
            )
            for q in range(QUARTERS):
                xbuf[pl.ds(part * rows, rows), pl.ds(q * width, width)] = turned[
                    q * rows : (q + 1) * rows
                ]
        step = min(256, hidden_width)

        @pl.loop(0, hidden_width // step)
        def _(n):
            cols = pl.ds(pl.multiple_of(n * step, step), step)
            gate_pre = jnp.dot(xbuf[...], gate[:, cols], preferred_element_type=jnp.float32)
            up_pre = jnp.dot(xbuf[...], up[:, cols], preferred_element_type=jnp.float32)
            hbuf[:, cols] = activate(gate_pre, up_pre).astype(jnp.bfloat16)

        out_step = min(512, half_model)

        @pl.loop(0, half_model // out_step)
        def _(n):
            for side in range(2):
                cols = pl.ds(
                    pl.multiple_of(side * half_model + n * out_step, out_step), out_step
                )
                here = pl.ds(pl.multiple_of(n * out_step, out_step), out_step)
                part_sum = jnp.dot(
                    hbuf[...], down[:, cols], preferred_element_type=jnp.float32
                ).astype(jnp.bfloat16)
                for part in range(4):
                    pbuf[g, part, side, :, here] = part_sum[part * rows : (part + 1) * rows]

        for side in range(2):
            far_half(side, g).start()
        for side in range(2):
            plain_half(side, g).start()

    def stage_e(g):
        for side in range(2):
            far_half(side, g).wait_recv()
            pbuf[g, 2 - side, side] = (
                pbuf[g, 2 - side, side].astype(jnp.float32) + rbuf[side, g].astype(jnp.float32)
            ).astype(jnp.bfloat16)
            added_half(side, g).start()

    def stage_f(g):
        for side in range(2):
            plain_half(side, g).wait_recv()
            added_half(side, g).wait_recv()
        quarters = []
        for h in range(2):
            total = (
                pbuf[g, 0, h].astype(jnp.float32)
                + sbuf[0, h, g].astype(jnp.float32)
                + sbuf[1, h, g].astype(jnp.float32)
            ).astype(jnp.bfloat16)
            quarters += [total[:, :width], total[:, width:]]
        stacked = jnp.concatenate(quarters, axis=0)
        ret[g] = (
            jnp.dot(perm_back[...], stacked, preferred_element_type=jnp.float32)
            .astype(jnp.bfloat16)
            .reshape(4, block_rows, width)
        )

    def near_back(g, sign, cs):
        zt = chip_at(-g - 1) if sign == 0 else chip_at(g + 1)
        return remote(
            ret.at[g, 2 * sign + cs],
            back.at[me],
            rs.at[4 * g + 2 * sign + cs],
            rr.at[4 * g + 2 * sign + c],
            at_z(zt, cs),
        )

    def far_back(cs):
        return remote(
            ret.at[last, 2 + cs],
            back.at[me],
            rs.at[4 * last + 2 + cs],
            rr.at[4 * last + 2 + c],
            at_z(chip_at(half), cs),
        )

    def partner_back():
        return remote(
            ret.at[last, 1 - c], back.at[me], rs.at[4 * last], rr.at[4 * last], at_z(z, 1 - c)
        )

    def stage_h(g):
        @pl.when(g < last)
        def _():
            for cs in range(CORES):
                for sign in range(2):
                    near_back(g, sign, cs).start()

        @pl.when(g == last)
        def _():
            for cs in range(CORES):
                far_back(cs).start()
            partner_back().start()
            back[me] = ret[last, c]

    @pl.loop(0, groups + 4)
    def _(i):
        @pl.when(i >= 4)
        def _():
            stage_f(i - 4)

        @pl.when(i >= 4)
        def _():
            stage_h(i - 4)

        @pl.when((i >= 3) & (i < groups + 3))
        def _():
            stage_e(i - 3)

        @pl.when((i >= 2) & (i < groups + 2))
        def _():
            stage_c(i - 2)

        @pl.when((i >= 1) & (i < groups + 1))
        def _():
            stage_b(i - 1)

        @pl.when(i < groups)
        def _():
            stage_a(i)

    partner_out().wait_send()
    partner_back().wait_send()
    partner_back().wait_recv()
    for ct in range(CORES):
        far_out(ct).wait_send()
        far_back(ct).wait_send()

    def back_arrived(g, j):
        return remote(ret.at[0, 0], back.at[0], rs.at[0], rr.at[4 * g + j], at_z(z, 1 - c))

    for j in (2, 3):
        back_arrived(last, j).wait_recv()

    @pl.loop(0, last)
    def _(g):
        for sign in range(2):
            for ct in range(CORES):
                near_out(g + 1, sign, ct).wait_send()
                near_back(g, sign, ct).wait_send()
        for j in range(4):
            back_arrived(g, j).wait_recv()

    @pl.loop(0, groups)
    def _(g):
        for side in range(2):
            spread(side, g).wait_send()
            relay(side, g).wait_send()
            far_half(side, g).wait_send()
            plain_half(side, g).wait_send()
            added_half(side, g).wait_send()

    arrived_rows = back[...].reshape(slots, width)
    for q in range(QUARTERS):
        own = slice(q * rows_dev, (q + 1) * rows_dev)
        cols = slice(q * width, (q + 1) * width)
        total = hidden[:, cols]
        for k in range(TOP_K):
            total = total + route_weights[:, k : k + 1] * jnp.dot(
                picks[k, own], arrived_rows, preferred_element_type=f32
            )
        out[:, cols] = total.astype(bf16)

    @pl.loop(1, devices)
    def _(step):
        piece_out(step).wait_send()
        answer_out(step).wait_send()

    for side in range(2):
        proj_far_half(side).wait_send()
        proj_plain_half(side).wait_send()
        proj_added_half(side).wait_send()


def layer_stage(
    query_wide,
    key_wide,
    value_wide,
    decay_wide,
    query_narrow,
    key_narrow,
    value_narrow,
    decay_narrow,
    residual,
    out_wide,
    out_narrow,
    norm_gain,
    routes,
    route_weights,
    gate,
    up,
    down,
):
    length = query_wide.shape[0]
    chips = lax.axis_size("sp_0")
    devices = chips * CORES
    groups = chips // 2
    rows_dev, model_width = residual.shape
    width = model_width // QUARTERS
    hidden_width = gate.shape[1]
    capacity = max(2, 3 * rows_dev * TOP_K // (2 * devices))
    block_rows = QUARTERS * capacity
    rows = 4 * capacity
    slots = devices * block_rows
    table = regroup(capacity)
    decay = jnp.concatenate(
        [decay_wide, decay_narrow, jnp.zeros((length, 2), jnp.float32)], axis=1
    )
    positions = (lax.axis_index(SP) * length + jnp.arange(length, dtype=jnp.int32)).astype(
        jnp.float32
    )
    inverse = [
        rotary_base ** (-jnp.arange(size // 2, dtype=jnp.float32) / (size // 2))
        for size in (HEAD_WIDE, HEAD_NARROW)
    ]
    inverse = jnp.concatenate(inverse + [jnp.zeros((HEAD_NARROW // 2,), jnp.float32)])
    angles = positions[:, None] * inverse[None, :]
    turns = jnp.concatenate([jnp.cos(angles), jnp.sin(angles)], axis=1)
    vmem = pl.BlockSpec(memory_space=pltpu.VMEM)
    hbm = pl.BlockSpec(memory_space=pl.ANY)
    bf16 = jnp.bfloat16
    f32 = jnp.float32
    dma = pltpu.SemaphoreType.DMA
    piece_rows = 2 * HEAD_WIDE // devices
    moved = pltpu.VMEM((devices, piece_rows, 2 * HEAD_WIDE), bf16)
    heads = pltpu.VMEM(query_wide.shape, bf16)
    half = model_width // 2
    from_hbm = (
        query_wide,
        key_wide,
        value_wide,
        query_narrow,
        key_narrow,
        value_narrow,
        out_wide,
        out_narrow,
        residual,
        gate,
        up,
        down,
    )
    return pl.pallas_call(
        functools.partial(layer_kernel, chips),
        out_shape=jax.ShapeDtypeStruct(residual.shape, bf16),
        in_specs=[vmem] * 8 + [hbm] * 12,
        out_specs=vmem,
        scratch_shapes=[pltpu.VMEM(a.shape, bf16) for a in from_hbm]
        + [
            pltpu.VMEM((rows_dev, model_width), f32),
            pltpu.VMEM((QUARTERS * rows_dev, width), bf16),
            pltpu.VMEM((slots, QUARTERS * rows_dev), bf16),
            pltpu.VMEM((TOP_K, QUARTERS * rows_dev, slots), bf16),
            pltpu.VMEM((devices, block_rows, width), bf16),
            pltpu.VMEM((devices, block_rows, width), bf16),
            pltpu.VMEM((4, length, HEAD_WIDE), bf16),
            pltpu.VMEM((4, length, HEAD_WIDE), bf16),
            pltpu.VMEM((4, length, HEAD_WIDE), f32),
            pltpu.VMEM((length, 4 * HEAD_WIDE), bf16),
            moved,
            moved,
            moved,
            moved,
            pltpu.VMEM((4, 2, rows_dev, half), bf16),
            pltpu.VMEM((2, rows_dev, half), bf16),
            pltpu.VMEM((2, 2, rows_dev, half), bf16),
            pltpu.VMEM((4, groups, 4, block_rows, width), bf16),
            pltpu.VMEM((4 * rows, model_width), bf16),
            pltpu.VMEM((4 * rows, hidden_width), bf16),
            pltpu.VMEM((groups, 4, 2, rows, half), bf16),
            pltpu.VMEM((2, groups, rows, half), bf16),
            pltpu.VMEM((2, 2, groups, rows, half), bf16),
            pltpu.VMEM((groups, 4, block_rows, width), bf16),
            dma((12,)),
            dma((devices,)),
            dma((devices,)),
            dma((devices,)),
            dma((devices,)),
            dma((2,)),
            dma((2,)),
            dma((2, 2)),
            dma((2, 2)),
            dma((4 * groups,)),
            dma((4 * groups,)),
            dma((2, groups)),
            dma((2, groups)),
            dma((2, groups)),
            dma((2, groups)),
            dma((2, groups)),
            dma((2, groups)),
            dma((2, 2, groups)),
            dma((2, 2, groups)),
            dma((4 * groups,)),
            dma((4 * groups,)),
        ],
        compiler_params=pltpu.CompilerParams(
            collective_id=0, has_side_effects=True, vmem_limit_bytes=60 * 1024 * 1024
        ),
        name="layer_stage",
    )(
        decay,
        decay.T,
        turns,
        norm_gain[None, :],
        routes,
        route_weights,
        jnp.asarray(table, bf16),
        jnp.asarray(table.T, bf16),
        *from_hbm,
    )


def body(*arguments):
    return layer_stage(*arguments[:14], *(weight[0] for weight in arguments[14:]))


def solution(mesh):
    torus = Mesh(
        mesh.devices.reshape(mesh.shape["grp"], 16, 2, mesh.shape["tp"]),
        ("grp", "sp_0", "sp_1", "tp"),
    )
    in_specs = (
        P(GRP_SP, "tp"),
        P(GRP_SP, "tp"),
        P(GRP_SP, "tp"),
        P(GRP_SP, "tp"),
        P(GRP_SP, "tp"),
        P(GRP_SP, "tp"),
        P(GRP_SP, "tp"),
        P(GRP_SP, "tp"),
        P(GRP_SP_TP, None),
        P("tp", None),
        P("tp", None),
        P(),
        P(GRP_SP_TP, None),
        P(GRP_SP_TP, None),
        P(SP, None, "tp"),
        P(SP, None, "tp"),
        P(SP, "tp", None),
    )
    out_specs = P(GRP_SP_TP, None)
    return jax.shard_map(body, mesh=torus, in_specs=in_specs, out_specs=out_specs, check_vma=False)
```

time: 357 us -> 231 us (0.65)
  blocking collectives: 99.7 us -> 0 us
  Pallas kernels: 177 us -> 218 us
  matrix products: 18.9 us -> 0 us
  between operations: 14 us -> 0.03 us
  waiting for transfers between devices: 13 us -> 0 us
  other arithmetic: 14 us -> 3.29 us
  local copies, waits for them, and re-layouts: 13.6 us -> 5.59 us
  starting transfers between devices: 5.2 us -> 0 us
    all_gather x7 -> x0, blocking collectives: 99.7 us -> none  [prefix_by_axis(): lax.all_gather(part.astype(kind), axis)]
    pallas_call x1, Pallas kernels: 177 us -> 218 us  [layer_stage(): pl.pallas_call(functools.partial(layer_kernel, chips), out_shape=jax.Shap...]
    dot_general x11 -> x0, matrix products: 18.9 us -> none  [the longest x2 6.17 us: local_terms(): inner_part = jnp.einsum('hts,she->the', scores, value_f)]
    all_to_all x1 -> x0, waiting for transfers between devices: 13 us -> none  [sent_and_summed(): lax.all_to_all(pieces, axis, split_axis=0, concat_axis=0, tiled=True)]
    all_to_all x1 -> x0, starting transfers between devices: 5.2 us -> none  [sent_and_summed(): lax.all_to_all(pieces, axis, split_axis=0, concat_axis=0, tiled=True)]
    another operation x7 -> x0, other arithmetic: 3.85 us -> none
  transfers between devices with their start and end apart: 2 -> 0, of which waited for: 1 -> 0; matrix products, arithmetic and copies ran while one was open for 6% -> 0% of each run, Pallas kernels for 0% -> 0%
where the time goes in v3:
time: 231 us; the launch traced here: 227 us
  Pallas kernels  218 us (94%)
  local copies, waits for them, and re-layouts  5.59 us (2%)
  other arithmetic  3.29 us (1%)
    pallas_call x1, Pallas kernels, layer_stage(): pl.pallas_call(functools.partial(layer_kernel, chips), out_shape=jax.Shap...  218 us
    unnamed x3, local copies, waits for them, and re-layouts  4.69 us

profile of v3, /device:TPU:33, one launch (start us, length us, event | category | flops | bytes accessed | tf_op | source)
XLA Modules:
  0.0 227.3 jit_solution(4731480566419979095)
XLA Ops:
  0.0 0.1 pad.7.clone
  0.1 0.1 pad_maximum_fusion.1
  0.2 1.4 fusion
  1.6 1.4 copy.21.routes
  3.0 1.4 copy.22.route_weights
  4.4 0.8 copy.20.decay
  5.2 1.0 multiply_cosine_fusion
  6.2 0.8 pad_maximum_fusion.turns
  7.0 218.4 %layer_stage.1 = bf16[128,2048]{1,0:T(8,128)(2,1)} custom-call(f32[512,8]{1,0:T(8,128)} %copy.20.decay, f32[8,512]{1,0:T(8,128)} %get-tuple-element.5.decay_t, f32[512,256]{1,0:T(8,128)} %pad_maximum_fusion.turns, f32[1,2048]{1,0:T(1,128)} %bitcast.9, s32[128,2]{1,0:T(8,128)} %copy.21.routes, f32[128,2]{1,0:T(8,128)} %copy.22.route_weights, ...), custom_call_target="tpu_custom_call" | custom-call | tf_op jit(solution)/shard_map/layer_stage/pallas_call | solution.py:935
  225.4 1.9 copy.24
  (5 shorter events, 0.0 us)

commit v4 on v3

--- a/solution.py
+++ b/solution.py
@@ -68,9 +68,10 @@
 
 def layer_kernel(
     chips,
-    decay,
-    decay_t,
-    turns,
+    decay_wide,
+    decay_narrow,
+    near_hbm,
+    block_turns,
     gain,
     routes,
     route_weights,
@@ -101,6 +102,7 @@
     gate,
     up,
     down,
+    near,
     hidden,
     parted,
     chosen,
@@ -173,6 +175,7 @@
         pltpu.make_async_copy(source, target, load_sem.at[n])
         for n, (source, target) in enumerate(
             (
+                (near_hbm, near),
                 (key_wide_hbm, key_wide),
                 (key_narrow_hbm, key_narrow),
                 (value_wide_hbm, value_wide),
@@ -188,7 +191,7 @@
             )
         )
     ]
-    for load in loads[:6]:
+    for load in loads[:7]:
         load.start()
 
     barrier = pltpu.get_barrier_semaphore()
@@ -199,17 +202,25 @@
     def _(step):
         pl.semaphore_signal(barrier, inc=1, device_id=peer(step)[1], device_id_type=MESH)
 
-    for load in loads[6:]:
+    for load in loads[7:]:
         load.start()
 
     square = (length, length)
     below = (rows_of(square) >= lanes_of(square)).astype(f32).astype(bf16)
-    cum = sum(dot_f32(below, term, ((1,), (0,))) for term in in_three(decay[...]))
-    cum_t = sum(dot_f32(term, below, ((1,), (1,))) for term in in_three(decay_t[...]))
+    decay_t = jnp.concatenate(
+        [decay_wide[...], decay_narrow[...], jnp.zeros((2, length), f32)], axis=0
+    )
+    terms = in_three(decay_t)
+    cum = sum(dot_f32(below, term, ((1,), (1,))) for term in terms)
+    cum_t = sum(dot_f32(term, below, ((1,), (1,))) for term in terms)
 
     table_lane = lanes_of((length, lane))
-    cos_all = turns[:, :lane]
-    sin_all = turns[:, lane:]
+    loads[0].wait()
+    start = block_turns[me]
+    start_cos = start[:, :lane]
+    start_sin = start[:, lane:]
+    cos_all = near[:, :lane] * start_cos - near[:, lane:] * start_sin
+    sin_all = near[:, lane:] * start_cos + near[:, :lane] * start_sin
     low = table_lane < HEAD_WIDE // 2
 
     def wide_table(table):
@@ -261,7 +272,7 @@
     unit_shape = (lane, lane)
     unit_low_row = rows_of(unit_shape) < HEAD_NARROW
     unit_low_lane = lanes_of(unit_shape) < HEAD_NARROW
-    for load in loads[:4]:
+    for load in loads[1:5]:
         load.wait()
     local = []
     for unit in range(units):
@@ -323,7 +334,7 @@
 
     arrived[me] = pieces[me]
 
-    for load in loads[4:6]:
+    for load in loads[5:7]:
         load.wait()
     for unit in range(units):
         qbuf[unit] = turned(query_wide if unit < 2 else query_narrow, unit).astype(bf16)
@@ -421,7 +432,7 @@
     model_width = out_wide.shape[1]
     proj_half = model_width // 2
 
-    for load in loads[6:9]:
+    for load in loads[7:10]:
         load.wait()
 
     def x_copy(src, dst, send_sem, recv_sem, side):
@@ -483,25 +494,29 @@
     experts = devices
     one_hots = []
     for k in range(TOP_K):
-        wanted = jnp.broadcast_to(routes[:, k : k + 1], (rows_dev, experts))
-        one_hots.append((wanted == lanes_of((rows_dev, experts))).astype(f32))
+        wanted = jnp.broadcast_to(routes[k : k + 1, :], (experts, rows_dev))
+        one_hots.append((wanted == rows_of((experts, rows_dev))).astype(f32))
     rows_square = (rows_dev, rows_dev)
-    above = (rows_of(rows_square) > lanes_of(rows_square)).astype(f32).astype(bf16)
+    earlier = (rows_of(rows_square) < lanes_of(rows_square)).astype(f32).astype(bf16)
     diagonal = rows_of(rows_square) == lanes_of(rows_square)
-    before = jnp.zeros((1, experts), f32)
+
+    def stood_up(row):
+        return jnp.sum(
+            jnp.where(diagonal, jnp.broadcast_to(row, rows_square), 0.0), axis=1, keepdims=True
+        )
+
+    before = jnp.zeros((experts, 1), f32)
     parts = QUARTERS * rows_dev
     slots = send.shape[0] * send.shape[1]
     capacity = send.shape[1] // QUARTERS
     width = send.shape[2]
     picked_rows = []
     for k in range(TOP_K):
-        ahead = dot_f32(above, one_hots[k].astype(bf16), ((1,), (0,))) + before
-        rank = jnp.sum(ahead * one_hots[k], axis=1, keepdims=True)
-        before = before + jnp.sum(one_hots[k], axis=0, keepdims=True)
-        place = routes[:, k : k + 1].astype(f32) * float(QUARTERS * capacity) + rank
-        across = jnp.sum(
-            jnp.where(diagonal, jnp.broadcast_to(place, rows_square), 0.0), axis=0, keepdims=True
-        )
+        ahead = dot_f32(one_hots[k].astype(bf16), earlier, ((1,), (0,))) + before
+        rank = jnp.sum(ahead * one_hots[k], axis=0, keepdims=True)
+        before = before + jnp.sum(one_hots[k], axis=1, keepdims=True)
+        across = routes[k : k + 1, :].astype(f32) * float(QUARTERS * capacity) + rank
+        place = stood_up(across)
         picked_rows.append(
             jnp.concatenate([across + float(q * capacity) for q in range(QUARTERS)], axis=1)
         )
@@ -610,7 +625,7 @@
     for ct in range(CORES):
         far_out(ct).start()
     gbuf[0, last, c] = send[me]
-    for load in loads[9:]:
+    for load in loads[10:]:
         load.wait()
 
     def z_arrived(g, j):
@@ -844,15 +859,16 @@
             added_half(side, g).wait_send()
 
     arrived_rows = back[...].reshape(slots, width)
+    shares = [stood_up(route_weights[k : k + 1, :]) for k in range(TOP_K)]
     for q in range(QUARTERS):
         own = slice(q * rows_dev, (q + 1) * rows_dev)
         cols = slice(q * width, (q + 1) * width)
         total = hidden[:, cols]
         for k in range(TOP_K):
-            total = total + route_weights[:, k : k + 1] * jnp.dot(
+            total = total + shares[k] * jnp.dot(
                 picks[k, own], arrived_rows, preferred_element_type=f32
             )
-        out[:, cols] = total.astype(bf16)
+        out[:, cols] = total
 
     @pl.loop(1, devices)
     def _(step):
@@ -863,6 +879,21 @@
         proj_far_half(side).wait_send()
         proj_plain_half(side).wait_send()
         proj_added_half(side).wait_send()
+
+
+def turn_tables(length, blocks):
+    inverse = [
+        rotary_base ** (-np.arange(size // 2) / (size // 2)) for size in (HEAD_WIDE, HEAD_NARROW)
+    ]
+    inverse = np.concatenate(inverse + [np.zeros(HEAD_NARROW // 2)])
+
+    def table(positions):
+        angles = positions[:, None] * inverse[None, :]
+        return jnp.asarray(
+            np.concatenate([np.cos(angles), np.sin(angles)], axis=1), jnp.float32
+        )
+
+    return table(np.arange(length)), table(np.arange(blocks) * length)[:, None, :]
 
 
 def layer_stage(
@@ -896,19 +927,7 @@
     rows = 4 * capacity
     slots = devices * block_rows
     table = regroup(capacity)
-    decay = jnp.concatenate(
-        [decay_wide, decay_narrow, jnp.zeros((length, 2), jnp.float32)], axis=1
-    )
-    positions = (lax.axis_index(SP) * length + jnp.arange(length, dtype=jnp.int32)).astype(
-        jnp.float32
-    )
-    inverse = [
-        rotary_base ** (-jnp.arange(size // 2, dtype=jnp.float32) / (size // 2))
-        for size in (HEAD_WIDE, HEAD_NARROW)
-    ]
-    inverse = jnp.concatenate(inverse + [jnp.zeros((HEAD_NARROW // 2,), jnp.float32)])
-    angles = positions[:, None] * inverse[None, :]
-    turns = jnp.concatenate([jnp.cos(angles), jnp.sin(angles)], axis=1)
+    near, block_turns = turn_tables(length, devices)
     vmem = pl.BlockSpec(memory_space=pltpu.VMEM)
     hbm = pl.BlockSpec(memory_space=pl.ANY)
     bf16 = jnp.bfloat16
@@ -934,11 +953,12 @@
     )
     return pl.pallas_call(
         functools.partial(layer_kernel, chips),
-        out_shape=jax.ShapeDtypeStruct(residual.shape, bf16),
-        in_specs=[vmem] * 8 + [hbm] * 12,
+        out_shape=jax.ShapeDtypeStruct(residual.shape, f32),
+        in_specs=[vmem] * 2 + [hbm] + [vmem] * 6 + [hbm] * 12,
         out_specs=vmem,
         scratch_shapes=[pltpu.VMEM(a.shape, bf16) for a in from_hbm]
         + [
+            pltpu.VMEM(near.shape, f32),
             pltpu.VMEM((rows_dev, model_width), f32),
             pltpu.VMEM((QUARTERS * rows_dev, width), bf16),
             pltpu.VMEM((slots, QUARTERS * rows_dev), bf16),
@@ -963,7 +983,7 @@
             pltpu.VMEM((2, groups, rows, half), bf16),
             pltpu.VMEM((2, 2, groups, rows, half), bf16),
             pltpu.VMEM((groups, 4, block_rows, width), bf16),
-            dma((12,)),
+            dma((13,)),
             dma((devices,)),
             dma((devices,)),
             dma((devices,)),
@@ -990,16 +1010,17 @@
         ),
         name="layer_stage",
     )(
-        decay,
-        decay.T,
-        turns,
+        decay_wide.T,
+        decay_narrow.T,
+        near,
+        block_turns,
         norm_gain[None, :],
-        routes,
-        route_weights,
+        routes.T,
+        route_weights.T,
         jnp.asarray(table, bf16),
         jnp.asarray(table.T, bf16),
         *from_hbm,
-    )
+    ).astype(bf16)
 
 
 def body(*arguments):

time: 231 us -> 222 us (0.961)
  local copies, waits for them, and re-layouts: 5.59 us -> 0 us
    unnamed x3 -> x0, local copies, waits for them, and re-layouts: 4.69 us -> none
where the time goes in v4:
time: 222 us; the launch traced here: 219 us
  Pallas kernels  217 us (98%)
    pallas_call x1, Pallas kernels, layer_stage(): pl.pallas_call(functools.partial(layer_kernel, chips), out_shape=jax.Shap...  217 us

profile of v4, /device:TPU:33, one launch (start us, length us, event | category | flops | bytes accessed | tf_op | source)
XLA Modules:
  0.0 219.5 jit_solution(10074180303814874844)
XLA Ops:
  0.0 217.4 %layer_stage.1 = f32[128,2048]{1,0:T(8,128)} custom-call(f32[2,512]{1,0:T(2,128)} %bitcast.13, f32[4,512]{1,0:T(4,128)} %bitcast.11, f32[512,256]{1,0:T(8,128)} %constant.6.clone.near_hbm, f32[32,1,256]{2,1,0:T(1,128)} %constant.16.block_turns, f32[1,2048]{1,0:T(1,128)} %bitcast.12, s32[2,128]{1,0:T(2,128)} %bitcast.14, f32[2,128]{1,0:T(2,128)} %bitcast.15, ...), custom_call_target="tpu_custom_call" | custom-call | tf_op jit(solution)/shard_map/layer_stage/pallas_call | solution.py:954
  217.4 2.1 convert_element_type.3

commit v5 on v4

--- a/solution.py
+++ b/solution.py
@@ -117,9 +117,14 @@
     arrived,
     answers,
     states,
-    proj,
-    proj_far,
-    proj_sum,
+    proj_a,
+    far_a,
+    sum_a,
+    proj_b,
+    far_b,
+    sum_b,
+    send_scale,
+    gscale,
     gbuf,
     xbuf,
     hbuf,
@@ -202,9 +207,6 @@
     def _(step):
         pl.semaphore_signal(barrier, inc=1, device_id=peer(step)[1], device_id_type=MESH)
 
-    for load in loads[7:]:
-        load.start()
-
     square = (length, length)
     below = (rows_of(square) >= lanes_of(square)).astype(f32).astype(bf16)
     decay_t = jnp.concatenate(
@@ -332,6 +334,8 @@
     def _(step):
         piece_out(step).start()
 
+    for load in loads[7:]:
+        load.start()
     arrived[me] = pieces[me]
 
     for load in loads[5:7]:
@@ -397,6 +401,50 @@
     for unit in range(2, units):
         within(unit)
 
+    rows_dev = residual.shape[0]
+    model_width = out_wide.shape[1]
+    experts = devices
+    one_hots = []
+    for k in range(TOP_K):
+        wanted = jnp.broadcast_to(routes[k : k + 1, :], (experts, rows_dev))
+        one_hots.append((wanted == rows_of((experts, rows_dev))).astype(f32))
+    rows_square = (rows_dev, rows_dev)
+    earlier = (rows_of(rows_square) < lanes_of(rows_square)).astype(f32).astype(bf16)
+    diagonal = rows_of(rows_square) == lanes_of(rows_square)
+
+    def stood_up(row):
+        return jnp.sum(
+            jnp.where(diagonal, jnp.broadcast_to(row, rows_square), 0.0), axis=1, keepdims=True
+        )
+
+    before = jnp.zeros((experts, 1), f32)
+    parts = QUARTERS * rows_dev
+    slots = send.shape[0] * send.shape[1]
+    capacity = send.shape[1] // QUARTERS
+    width = send.shape[2]
+    picked_rows = []
+    ranks = []
+    places = []
+    for k in range(TOP_K):
+        ahead = dot_f32(one_hots[k].astype(bf16), earlier, ((1,), (0,))) + before
+        rank = jnp.sum(ahead * one_hots[k], axis=0, keepdims=True)
+        before = before + jnp.sum(one_hots[k], axis=1, keepdims=True)
+        across = routes[k : k + 1, :].astype(f32) * float(QUARTERS * capacity) + rank
+        place = stood_up(across)
+        picked_rows.append(
+            jnp.concatenate([across + float(q * capacity) for q in range(QUARTERS)], axis=1)
+        )
+        ranks.append(rank)
+        places.append(place)
+    step_rows = slots // 4
+
+    @pl.loop(0, 4)
+    def _(n):
+        first = pl.multiple_of(n * step_rows, step_rows)
+        slot = (rows_of((step_rows, parts)) + first).astype(f32)
+        hit = (slot == picked_rows[0]) | (slot == picked_rows[1])
+        chosen[pl.ds(first, step_rows)] = hit.astype(f32).astype(bf16)
+
     @pl.loop(1, devices)
     def _(step):
         answer_out(step).wait_recv()
@@ -428,10 +476,12 @@
             centered * lax.rsqrt(spread + norm_eps)
         ).astype(bf16)
 
-    rows_dev = length // nx
-    model_width = out_wide.shape[1]
-    proj_half = model_width // 2
-
+    half_model = model_width // 2
+    first_cols = model_width // 4
+    sub_width = width // 4
+    starts = (0, first_cols)
+    halves = (first_cols // 2, (model_width - first_cols) // 2)
+    sums = ((proj_a, far_a, sum_a), (proj_b, far_b, sum_b))
     for load in loads[7:10]:
         load.wait()
 
@@ -445,131 +495,95 @@
             device_id_type=MESH,
         )
 
-    def proj_far_half(side):
-        return x_copy(proj.at[3, side], proj_far.at[side], pds.at[side], pdr.at[side], side)
-
-    def proj_plain_half(side):
+    def proj_far_half(n, side):
         return x_copy(
-            proj.at[2 - side, 1 - side], proj_sum.at[side, 1 - side], pes.at[side, 0], per.at[side, 0], side
-        )
-
-    def proj_added_half(side):
+            sums[n][0].at[3, side], sums[n][1].at[side], pds.at[n, side], pdr.at[n, side], side
+        )
+
+    def proj_plain_half(n, side):
         return x_copy(
-            proj.at[2 - side, side], proj_sum.at[side, side], pes.at[side, 1], per.at[side, 1], side
-        )
-
-    out_step = min(512, proj_half)
-
-    def project(part, side):
+            sums[n][0].at[2 - side, 1 - side],
+            sums[n][2].at[side, 1 - side],
+            pes.at[n, side, 0],
+            per.at[n, side, 0],
+            side,
+        )
+
+    def proj_added_half(n, side):
+        return x_copy(
+            sums[n][0].at[2 - side, side],
+            sums[n][2].at[side, side],
+            pes.at[n, side, 1],
+            per.at[n, side, 1],
+            side,
+        )
+
+    def project(n, part, side):
         target = (x, left, right, lax.rem(x + 2, nx))[part]
         own_rows = pl.ds(pl.multiple_of(target * rows_dev, rows_dev), rows_dev)
-
-        @pl.loop(0, proj_half // out_step)
-        def _(n):
-            cols = pl.ds(pl.multiple_of(side * proj_half + n * out_step, out_step), out_step)
-            here = pl.ds(pl.multiple_of(n * out_step, out_step), out_step)
+        step = min(256, halves[n])
+
+        @pl.loop(0, halves[n] // step)
+        def _(i):
+            cols = pl.ds(pl.multiple_of(starts[n] + side * halves[n] + i * step, step), step)
+            here = pl.ds(pl.multiple_of(i * step, step), step)
             both = jnp.dot(
                 mixed[own_rows, : 2 * lane], out_wide[:, cols], preferred_element_type=f32
             ) + jnp.dot(
                 mixed[own_rows, 2 * lane :], out_narrow[:, cols], preferred_element_type=f32
             )
-            proj[part, side, :, here] = both.astype(bf16)
-
-    for side in range(2):
-        project(3, side)
-        proj_far_half(side).start()
-    for side in range(2):
-        project(2 - side, 1 - side)
-        proj_plain_half(side).start()
-    for side in range(2):
-        project(2 - side, side)
-    for side in range(2):
-        project(0, side)
-    for side in range(2):
-        proj_far_half(side).wait_recv()
-        proj[2 - side, side] = (
-            proj[2 - side, side].astype(f32) + proj_far[side].astype(f32)
-        ).astype(bf16)
-        proj_added_half(side).start()
-    experts = devices
-    one_hots = []
-    for k in range(TOP_K):
-        wanted = jnp.broadcast_to(routes[k : k + 1, :], (experts, rows_dev))
-        one_hots.append((wanted == rows_of((experts, rows_dev))).astype(f32))
-    rows_square = (rows_dev, rows_dev)
-    earlier = (rows_of(rows_square) < lanes_of(rows_square)).astype(f32).astype(bf16)
-    diagonal = rows_of(rows_square) == lanes_of(rows_square)
-
-    def stood_up(row):
-        return jnp.sum(
-            jnp.where(diagonal, jnp.broadcast_to(row, rows_square), 0.0), axis=1, keepdims=True
-        )
-
-    before = jnp.zeros((experts, 1), f32)
-    parts = QUARTERS * rows_dev
-    slots = send.shape[0] * send.shape[1]
-    capacity = send.shape[1] // QUARTERS
-    width = send.shape[2]
-    picked_rows = []
-    for k in range(TOP_K):
-        ahead = dot_f32(one_hots[k].astype(bf16), earlier, ((1,), (0,))) + before
-        rank = jnp.sum(ahead * one_hots[k], axis=0, keepdims=True)
-        before = before + jnp.sum(one_hots[k], axis=1, keepdims=True)
-        across = routes[k : k + 1, :].astype(f32) * float(QUARTERS * capacity) + rank
-        place = stood_up(across)
-        picked_rows.append(
-            jnp.concatenate([across + float(q * capacity) for q in range(QUARTERS)], axis=1)
-        )
+            sums[n][0][part, side, :, here] = both.astype(bf16)
+
+    def add_far(n):
+        own = sums[n][0]
+        for side in range(2):
+            proj_far_half(n, side).wait_recv()
+            own[2 - side, side] = (
+                own[2 - side, side].astype(f32) + sums[n][1][side].astype(f32)
+            ).astype(bf16)
+            proj_added_half(n, side).start()
+
+    def finish_sum(n):
+        own, _, came = sums[n]
+        squares = jnp.zeros((rows_dev, 1), f32)
+        for side in range(2):
+            proj_plain_half(n, side).wait_recv()
+            proj_added_half(n, side).wait_recv()
+        for h in range(2):
+            cols = slice(starts[n] + h * halves[n], starts[n] + (h + 1) * halves[n])
+            stream = residual[:, cols].astype(f32) + (
+                own[0, h].astype(f32) + came[0, h].astype(f32) + came[1, h].astype(f32)
+            )
+            hidden[:, cols] = stream
+            squares = squares + jnp.sum(stream * stream, axis=1, keepdims=True)
+        return squares
+
+    step_experts = experts // 4
+
+    def fill_send(n):
+        here = slice(0, sub_width) if n == 0 else slice(sub_width, width)
+        size = sub_width if n == 0 else width - sub_width
         for q in range(QUARTERS):
-            own = slice(q * rows_dev, (q + 1) * rows_dev)
-            wanted = jnp.broadcast_to(place + float(q * capacity), (rows_dev, slots))
-            picks[k, own] = (
-                (wanted == lanes_of((rows_dev, slots)).astype(f32)).astype(f32).astype(bf16)
+            cols = slice(starts[n] + q * size, starts[n] + (q + 1) * size)
+            parted[q * rows_dev : (q + 1) * rows_dev, here] = (
+                hidden[:, cols] * gain[:, cols]
+            ).astype(bf16)
+
+        @pl.loop(0, 4)
+        def _(i):
+            first = pl.multiple_of(i * step_rows, step_rows)
+            taken = jnp.dot(
+                chosen[pl.ds(first, step_rows)], parted[:, here], preferred_element_type=f32
+            ).astype(bf16)
+            send[pl.ds(i * step_experts, step_experts), :, here] = taken.reshape(
+                step_experts, QUARTERS * capacity, size
             )
-    step_rows = slots // 4
-
-    @pl.loop(0, 4)
-    def _(n):
-        first = pl.multiple_of(n * step_rows, step_rows)
-        slot = (rows_of((step_rows, parts)) + first).astype(f32)
-        hit = (slot == picked_rows[0]) | (slot == picked_rows[1])
-        chosen[pl.ds(first, step_rows)] = hit.astype(f32).astype(bf16)
-
-    for side in range(2):
-        proj_plain_half(side).wait_recv()
-        proj_added_half(side).wait_recv()
-    squares = jnp.zeros((rows_dev, 1), f32)
-    for h in range(2):
-        cols = slice(h * proj_half, (h + 1) * proj_half)
-        stream = residual[:, cols].astype(f32) + (
-            proj[0, h].astype(f32) + proj_sum[0, h].astype(f32) + proj_sum[1, h].astype(f32)
-        )
-        hidden[:, cols] = stream
-        squares = squares + jnp.sum(stream * stream, axis=1, keepdims=True)
-    scale_row = lax.rsqrt(squares * (1.0 / model_width) + norm_eps)
-    for q in range(QUARTERS):
-        cols = slice(q * width, (q + 1) * width)
-        parted[q * rows_dev : (q + 1) * rows_dev] = (
-            hidden[:, cols] * scale_row * gain[:, cols]
-        ).astype(bf16)
-    step_experts = experts // 4
-
-    @pl.loop(0, 4)
-    def _(n):
-        first = pl.multiple_of(n * step_rows, step_rows)
-        taken = jnp.dot(
-            chosen[pl.ds(first, step_rows)], parted[...], preferred_element_type=f32
-        ).astype(bf16)
-        send[pl.ds(n * step_experts, step_experts)] = taken.reshape(
-            step_experts, QUARTERS * capacity, width
-        )
 
     half = chips // 2
     groups = half
     last = groups - 1
     block_rows = send.shape[1]
     rows = 4 * capacity
-    half_model = QUARTERS * width // 2
     hidden_width = gate.shape[1]
 
     def remote(src, dst, send_sem, recv_sem, to):
@@ -588,85 +602,152 @@
     def chip_at(offset):
         return lax.rem(z + offset + chips, chips)
 
-    def partner_out():
+    def parts_of(piece, sender, taker):
+        if piece == 2:
+            return send_scale.at[sender], gscale.at[taker]
+        lanes = pl.ds(0, sub_width) if piece == 0 else pl.ds(sub_width, width - sub_width)
+        return send.at[sender, :, lanes], gbuf.at[taker + (slice(None), lanes)]
+
+    def partner_out(piece):
+        src, dst = parts_of(piece, z * CORES + 1 - c, (0, last, c))
+        return remote(src, dst, zs.at[piece, 4 * last], zr.at[piece, 4 * last], at_z(z, 1 - c))
+
+    def far_out(piece, ct):
+        zt = chip_at(half)
+        src, dst = parts_of(piece, zt * CORES + ct, (0, last, 2 + c))
         return remote(
-            send.at[z * CORES + 1 - c], gbuf.at[0, last, c], zs.at[4 * last], zr.at[4 * last],
-            at_z(z, 1 - c),
-        )
-
-    def far_out(ct):
-        zt = chip_at(half)
+            src, dst, zs.at[piece, 4 * last + 2 + ct], zr.at[piece, 4 * last + 2 + c], at_z(zt, ct)
+        )
+
+    def near_out(piece, d, sign, ct):
+        zt = chip_at(d) if sign == 0 else chip_at(-d)
+        src, dst = parts_of(piece, zt * CORES + ct, (0, d - 1, 2 * sign + c))
         return remote(
-            send.at[zt * CORES + ct],
-            gbuf.at[0, last, 2 + c],
-            zs.at[4 * last + 2 + ct],
-            zr.at[4 * last + 2 + c],
+            src,
+            dst,
+            zs.at[piece, 4 * (d - 1) + 2 * sign + ct],
+            zr.at[piece, 4 * (d - 1) + 2 * sign + c],
             at_z(zt, ct),
         )
 
-    def near_out(d, sign, ct):
-        zt = chip_at(d) if sign == 0 else chip_at(-d)
-        return remote(
-            send.at[zt * CORES + ct],
-            gbuf.at[0, d - 1, 2 * sign + c],
-            zs.at[4 * (d - 1) + 2 * sign + ct],
-            zr.at[4 * (d - 1) + 2 * sign + c],
-            at_z(zt, ct),
-        )
-
-    partner_out().start()
-
-    @pl.loop(1, half)
-    def _(d):
+    def dispatch(pieces_now):
+        for piece in pieces_now:
+            partner_out(piece).start()
+
+        @pl.loop(1, half)
+        def _(d):
+            for ct in range(CORES):
+                for sign in range(2):
+                    for piece in pieces_now:
+                        near_out(piece, d, sign, ct).start()
+
         for ct in range(CORES):
-            for sign in range(2):
-                near_out(d, sign, ct).start()
-
-    for ct in range(CORES):
-        far_out(ct).start()
+            for piece in pieces_now:
+                far_out(piece, ct).start()
+
+    for side in range(2):
+        project(0, 3, side)
+        proj_far_half(0, side).start()
+    for side in range(2):
+        project(0, 2 - side, 1 - side)
+        proj_plain_half(0, side).start()
+    for side in range(2):
+        project(0, 2 - side, side)
+    for side in range(2):
+        project(1, 3, side)
+    add_far(0)
+    for side in range(2):
+        proj_far_half(1, side).start()
+    for side in range(2):
+        project(1, 2 - side, 1 - side)
+        proj_plain_half(1, side).start()
+    for side in range(2):
+        project(0, 0, side)
+    squares = finish_sum(0)
+    fill_send(0)
+    dispatch((0,))
+    for side in range(2):
+        project(1, 2 - side, side)
+    add_far(1)
+    for side in range(2):
+        project(1, 0, side)
+    squares = squares + finish_sum(1)
+    scale_row = lax.rsqrt(squares * (1.0 / model_width) + norm_eps)
+    laid = jnp.sum(
+        jnp.where(diagonal, jnp.broadcast_to(scale_row, rows_square), 0.0), axis=0, keepdims=True
+    )
+    slot_scale = jnp.zeros((experts, lane), f32)
+    for k in range(TOP_K):
+        at_rank = jnp.broadcast_to(stood_up(ranks[k]), (rows_dev, lane)) == lanes_of(
+            (rows_dev, lane)
+        ).astype(f32)
+        for term in in_three(laid):
+            held = (one_hots[k] * term.astype(f32)).astype(bf16)
+            slot_scale = slot_scale + dot_f32(
+                held, at_rank.astype(f32).astype(bf16), ((1,), (0,))
+            )
+    for e in range(experts):
+        send_scale[e] = slot_scale[e : e + 1]
+    fill_send(1)
+    dispatch((2, 1))
     gbuf[0, last, c] = send[me]
+    gscale[0, last, c] = send_scale[me]
+    for k in range(TOP_K):
+        for q in range(QUARTERS):
+            own = slice(q * rows_dev, (q + 1) * rows_dev)
+            wanted = jnp.broadcast_to(places[k] + float(q * capacity), (rows_dev, slots))
+            picks[k, own] = (
+                (wanted == lanes_of((rows_dev, slots)).astype(f32)).astype(f32).astype(bf16)
+            )
     for load in loads[10:]:
         load.wait()
 
-    def z_arrived(g, j):
-        return remote(send.at[0], gbuf.at[0, g, j], zs.at[0], zr.at[4 * g + j], at_z(z, 1 - c))
-
-    def spread(side, g):
+    def z_arrived(piece, g, j):
+        src, dst = parts_of(piece, 0, (0, g, j))
+        return remote(src, dst, zs.at[piece, 0], zr.at[piece, 4 * g + j], at_z(z, 1 - c))
+
+    def spread(kind, side, g):
+        held = (gbuf, gscale)[kind]
         return remote(
-            gbuf.at[0, g],
-            gbuf.at[1 + side, g],
-            xs.at[side, g],
-            xr.at[side, g],
+            held.at[0, g],
+            held.at[1 + side, g],
+            xs.at[kind, side, g],
+            xr.at[kind, side, g],
             at_x(right if side == 0 else left),
         )
 
-    def relay(side, g):
+    def relay(kind, side, g):
+        held = (gbuf, gscale)[kind]
         return remote(
-            gbuf.at[1 + side, g, pl.ds(2 * side, 2)],
-            gbuf.at[3, g, pl.ds(2 * side, 2)],
-            ys.at[side, g],
-            yr.at[side, g],
+            held.at[1 + side, g, pl.ds(2 * side, 2)],
+            held.at[3, g, pl.ds(2 * side, 2)],
+            ys.at[kind, side, g],
+            yr.at[kind, side, g],
             at_x(right if side == 0 else left),
         )
 
     def stage_a(g):
         @pl.when(g < last)
         def _():
-            for j in range(4):
-                z_arrived(g, j).wait_recv()
+            for piece in range(3):
+                for j in range(4):
+                    z_arrived(piece, g, j).wait_recv()
 
         @pl.when(g == last)
         def _():
-            for j in (0, 2, 3):
-                z_arrived(g, j).wait_recv()
+            for piece in range(3):
+                for j in (0, 2, 3):
+                    z_arrived(piece, g, j).wait_recv()
 
         for side in range(2):
-            spread(side, g).start()
+            for kind in range(2):
+                spread(kind, side, g).start()
 
     def stage_b(g):
         for side in range(2):
-            spread(side, g).wait_recv()
-            relay(side, g).start()
+            for kind in range(2):
+                spread(kind, side, g).wait_recv()
+                relay(kind, side, g).start()
 
     def far_half(side, g):
         return remote(
@@ -697,16 +778,29 @@
 
     def stage_c(g):
         for side in range(2):
-            relay(side, g).wait_recv()
+            for kind in range(2):
+                relay(kind, side, g).wait_recv()
+        factors = []
+        factor_shape = (rows, lane)
         for part in range(4):
             block = gbuf[part, g].reshape(4 * block_rows, width)
-            turned = jnp.dot(perm[...], block, preferred_element_type=jnp.float32).astype(
+            turned_rows = jnp.dot(perm[...], block, preferred_element_type=jnp.float32).astype(
                 jnp.bfloat16
             )
+            rest = width - sub_width
             for q in range(QUARTERS):
-                xbuf[pl.ds(part * rows, rows), pl.ds(q * width, width)] = turned[
-                    q * rows : (q + 1) * rows
-                ]
+                taken = turned_rows[q * rows : (q + 1) * rows]
+                own = pl.ds(part * rows, rows)
+                xbuf[own, pl.ds(q * sub_width, sub_width)] = taken[:, :sub_width]
+                xbuf[own, pl.ds(first_cols + q * rest, rest)] = taken[:, sub_width:]
+            factor = jnp.zeros((rows, 1), f32)
+            for j in range(4):
+                place_in = rows_of(factor_shape) - j * capacity
+                mine = (lanes_of(factor_shape) == place_in) & (place_in < capacity)
+                came = jnp.broadcast_to(gscale[part, g, j], factor_shape)
+                factor = factor + jnp.sum(jnp.where(mine, came, 0.0), axis=1, keepdims=True)
+            factors.append(factor)
+        factor = jnp.concatenate(factors, axis=0)
         step = min(256, hidden_width)
 
         @pl.loop(0, hidden_width // step)
@@ -714,7 +808,7 @@
             cols = pl.ds(pl.multiple_of(n * step, step), step)
             gate_pre = jnp.dot(xbuf[...], gate[:, cols], preferred_element_type=jnp.float32)
             up_pre = jnp.dot(xbuf[...], up[:, cols], preferred_element_type=jnp.float32)
-            hbuf[:, cols] = activate(gate_pre, up_pre).astype(jnp.bfloat16)
+            hbuf[:, cols] = activate(factor * gate_pre, factor * up_pre).astype(jnp.bfloat16)
 
         out_step = min(512, half_model)
 
@@ -827,11 +921,13 @@
         def _():
             stage_a(i)
 
-    partner_out().wait_send()
+    for piece in range(3):
+        partner_out(piece).wait_send()
+        for ct in range(CORES):
+            far_out(piece, ct).wait_send()
     partner_back().wait_send()
     partner_back().wait_recv()
     for ct in range(CORES):
-        far_out(ct).wait_send()
         far_back(ct).wait_send()
 
     def back_arrived(g, j):
@@ -844,7 +940,8 @@
     def _(g):
         for sign in range(2):
             for ct in range(CORES):
-                near_out(g + 1, sign, ct).wait_send()
+                for piece in range(3):
+                    near_out(piece, g + 1, sign, ct).wait_send()
                 near_back(g, sign, ct).wait_send()
         for j in range(4):
             back_arrived(g, j).wait_recv()
@@ -852,8 +949,9 @@
     @pl.loop(0, groups)
     def _(g):
         for side in range(2):
-            spread(side, g).wait_send()
-            relay(side, g).wait_send()
+            for kind in range(2):
+                spread(kind, side, g).wait_send()
+                relay(kind, side, g).wait_send()
             far_half(side, g).wait_send()
             plain_half(side, g).wait_send()
             added_half(side, g).wait_send()
@@ -875,10 +973,11 @@
         piece_out(step).wait_send()
         answer_out(step).wait_send()
 
-    for side in range(2):
-        proj_far_half(side).wait_send()
-        proj_plain_half(side).wait_send()
-        proj_added_half(side).wait_send()
+    for n in range(2):
+        for side in range(2):
+            proj_far_half(n, side).wait_send()
+            proj_plain_half(n, side).wait_send()
+            proj_added_half(n, side).wait_send()
 
 
 def turn_tables(length, blocks):
@@ -973,9 +1072,14 @@
             moved,
             moved,
             moved,
-            pltpu.VMEM((4, 2, rows_dev, half), bf16),
-            pltpu.VMEM((2, rows_dev, half), bf16),
-            pltpu.VMEM((2, 2, rows_dev, half), bf16),
+            pltpu.VMEM((4, 2, rows_dev, half // 4), bf16),
+            pltpu.VMEM((2, rows_dev, half // 4), bf16),
+            pltpu.VMEM((2, 2, rows_dev, half // 4), bf16),
+            pltpu.VMEM((4, 2, rows_dev, half - half // 4), bf16),
+            pltpu.VMEM((2, rows_dev, half - half // 4), bf16),
+            pltpu.VMEM((2, 2, rows_dev, half - half // 4), bf16),
+            pltpu.VMEM((devices, 1, HEAD_WIDE), f32),
+            pltpu.VMEM((4, groups, 4, 1, HEAD_WIDE), f32),
             pltpu.VMEM((4, groups, 4, block_rows, width), bf16),
             pltpu.VMEM((4 * rows, model_width), bf16),
             pltpu.VMEM((4 * rows, hidden_width), bf16),
@@ -988,16 +1092,16 @@
             dma((devices,)),
             dma((devices,)),
             dma((devices,)),
-            dma((2,)),
-            dma((2,)),
             dma((2, 2)),
             dma((2, 2)),
-            dma((4 * groups,)),
-            dma((4 * groups,)),
-            dma((2, groups)),
-            dma((2, groups)),
-            dma((2, groups)),
-            dma((2, groups)),
+            dma((2, 2, 2)),
+            dma((2, 2, 2)),
+            dma((3, 4 * groups)),
+            dma((3, 4 * groups)),
+            dma((2, 2, groups)),
+            dma((2, 2, groups)),
+            dma((2, 2, groups)),
+            dma((2, 2, groups)),
             dma((2, groups)),
             dma((2, groups)),
             dma((2, 2, groups)),

time: 222 us -> 223 us (level)
  no operation moved by 1% of the time
where the time goes in v5:
time: 223 us; the launch traced here: 219 us
  Pallas kernels  217 us (97%)
    pallas_call x1, Pallas kernels, layer_stage(): pl.pallas_call(functools.partial(layer_kernel, chips), out_shape=jax.Shap...  217 us

profile of v5, /device:TPU:33, one launch (start us, length us, event | category | flops | bytes accessed | tf_op | source)
XLA Modules:
  0.0 219.1 jit_solution(4551221585975030192)
XLA Ops:
  0.0 217.0 %layer_stage.1 = f32[128,2048]{1,0:T(8,128)} custom-call(f32[2,512]{1,0:T(2,128)} %bitcast.13, f32[4,512]{1,0:T(4,128)} %bitcast.11, f32[512,256]{1,0:T(8,128)} %constant.6.clone.near_hbm, f32[32,1,256]{2,1,0:T(1,128)} %constant.16.block_turns, f32[1,2048]{1,0:T(1,128)} %bitcast.12, s32[2,128]{1,0:T(2,128)} %bitcast.14, f32[2,128]{1,0:T(2,128)} %bitcast.15, ...), custom_call_target="tpu_custom_call" | custom-call | tf_op jit(solution)/shard_map/layer_stage/pallas_call | solution.py:1053
  217.0 2.1 convert_element_type.3
